TPU v7x, 32 devices: a whole 2x2x4 slice. The times are simulated.
32 devices in a mesh: ep: 8 (over z, x), tp: 4 (over y, core).
Axes of the slice: x: 2, y: 2, z: 4, core: 2. Of those that a mesh axis runs over, the one named last changes fastest.
Arguments:
- queries: bfloat16 [2048, 8, 128], P('ep', 'tp'), may hold values from -256 to 256
- keys: bfloat16 [2048, 4, 128], P('ep', 'tp'), may hold values from -8 to 8
- values: bfloat16 [2048, 4, 128], P('ep', 'tp'), may hold values from -6 to 6
- attn_lambda: float32 [8], P('tp'), may hold values from 0.3 to 0.8
- head_gain: float32 [128], replicated, may hold values from 0.1 to 1.9
- w_out: bfloat16 [1024, 2048], replicated, may hold values from -0.1875 to 0.1875
- moe_rows: bfloat16 [4096, 2048], P('ep'), may hold values from -6 to 6
- moe_gain: float32 [2048], replicated, may hold values from 0.1 to 1.9
- routes: int32 [4096, 2], P('ep'), may hold values from 0 to 7, all different within a row; in each aligned block of 128 rows (0 to 127, 128 to 255, ...) at most 64 rows name the same one
- route_weights: float32 [4096, 2], P('ep'), may hold values from 0.1 to 1
- w_gate: bfloat16 [8, 2048, 1024], P('ep', None, 'tp'), may hold values from -0.125 to 0.125
- w_up: bfloat16 [8, 2048, 1024], P('ep', None, 'tp'), may hold values from -0.125 to 0.125
- w_down: bfloat16 [8, 1024, 2048], P('ep', 'tp'), may hold values from -0.1875 to 0.1875
Outputs:
- mixer_out: bfloat16 [2048, 2048], P(('ep', 'tp'))
- moe_out: bfloat16 [4096, 2048], P(('ep', 'tp'))
Inputs may be any that keep to these rules, and one draw needn't show every extreme that they name: `routes`: each row names 2 different experts. In each aligned block of 128 rows (the rows of moe_out that one device holds) no expert is named by more than 64 rows, a bound that some block reaches.
All inputs are finite; a program needn't handle non-finite values.
Results may differ from a plain program's by a relative error of at most 0.011.
Values may be sent and summed in bfloat16 or wider, within the bound.
A program may use at most 128 MiB of HBM per device.

v0:
```python
import functools

import jax
import jax.numpy as jnp
from jax import lax
from jax.experimental import pallas as pl
from jax.experimental.pallas import tpu as pltpu
from jax.sharding import PartitionSpec as P

EPSILON = 1e-06
MASKED = -1e30


def rms_scaled(values_f, gain):
    mean_sq = jnp.mean(values_f * values_f, axis=-1, keepdims=True)
    return values_f * lax.rsqrt(mean_sq + EPSILON) * gain


def expert_kernel(
    n,
    out_ref,
    near_ref,
    mine_ref,
    kv_ref,
    gate_ref,
    up_ref,
    down_ref,
    mix_ref,
    res_ref,
    kv_out,
    slots,
    part,
    pair_in,
    col_in,
    back,
    hidden_ref,
    acc,
    send_k,
    recv_k,
    send_a,
    recv_a,
    send_y,
    recv_y,
    send_c,
    recv_c,
    send_b,
    recv_b,
    send_p,
    recv_p,
    send_q,
    recv_q,
    send_r,
    recv_r,
    local_sem,
):
    me = lax.axis_index("ep")
    tp = lax.axis_index("tp")
    row = tp // 2
    col = tp % 2
    other_row = 1 - row
    other_col = 1 - col
    pair_peer = row * 2 + other_col
    row_peer = other_row * 2 + col
    own_blk = col * 2 + row
    far_blk = col * 2 + other_row
    slot_count = slots.shape[2]
    width = slots.shape[3]

    near = near_ref.shape[0]
    bits = [1 << b for b in range(n.bit_length() - 1)]

    def partner(d):
        total = 0
        for bit in bits:
            total = total + (me // bit + d // bit) % 2 * bit
        return total

    def remote(src, dst, ssem, rsem, ep_id, tp_id):
        return pltpu.make_async_remote_copy(
            src_ref=src,
            dst_ref=dst,
            send_sem=ssem,
            recv_sem=rsem,
            device_id=(ep_id, tp_id),
            device_id_type=pl.DeviceIdType.MESH,
        )

    barrier = pltpu.get_barrier_semaphore()

    @pl.loop(1, n)
    def _(d):
        pl.semaphore_signal(
            barrier, inc=1, device_id=(partner(d), tp), device_id_type=pl.DeviceIdType.MESH
        )

    for peer in (pair_peer, row_peer):
        pl.semaphore_signal(
            barrier, inc=1, device_id=(me, peer), device_id_type=pl.DeviceIdType.MESH
        )
    keep = pltpu.make_async_copy(kv_ref, kv_out.at[me], local_sem.at[4])
    keep.start()
    fills = [
        pltpu.make_async_copy(
            mine_ref.at[b], slots.at[0, (b % 2) * 2 + b // 2], local_sem.at[b]
        )
        for b in range(4)
    ]
    for fill in fills:
        fill.start()
    pl.semaphore_wait(barrier, n + 1)

    def copy_a(d):
        return remote(
            out_ref.at[d], slots.at[d, own_blk], send_a.at[d], recv_a.at[d], partner(d), tp
        )

    def copy_k(d):
        return remote(kv_ref, kv_out.at[me], send_k.at[d], recv_k.at[d], partner(d), tp)

    def copy_f(d):
        block = kv_out.at[partner(near)]
        return remote(block, block, send_k.at[d], recv_k.at[d], partner(d - near), tp)

    def copy_n(d):
        return remote(
            near_ref.at[d], slots.at[d, far_blk], send_y.at[d], recv_y.at[d], partner(d), tp
        )

    def copy_y(d):
        block = slots.at[d, own_blk]
        return remote(block, block, send_y.at[d], recv_y.at[d], me, row_peer)

    def copy_c(d):
        block = slots.at[d, own_blk]
        return remote(block, block, send_c.at[d], recv_c.at[d], me, pair_peer)

    def copy_b(d):
        block = slots.at[d, far_blk]
        return remote(block, block, send_b.at[d], recv_b.at[d], me, pair_peer)

    def copy_p(d):
        return remote(
            part.at[d, pl.ds(other_col * 2, 2)],
            pair_in.at[d],
            send_p.at[d],
            recv_p.at[d],
            me,
            pair_peer,
        )

    def copy_q(d):
        return remote(part.at[d, far_blk], col_in.at[d], send_q.at[d], recv_q.at[d], me, row_peer)

    def copy_r(d):
        return remote(
            part.at[d, own_blk], back.at[d], send_r.at[d], recv_r.at[d], partner(d), tp
        )

    @pl.loop(1, n)
    def _(d):
        copy_a(d).start()

        @pl.when(d < near)
        def _():
            copy_n(d).start()

    copy_k(near).start()

    @pl.loop(1, near)
    def _(d):
        copy_k(d).start()

    for fill in fills:
        fill.wait()

    def merge(index, other):
        rows = part.at[index]
        step = min(512, width)

        @pl.loop(0, width // step)
        def _(c):
            cols = pl.ds(pl.multiple_of(c * step, step), step)
            rows[:, cols] = (
                rows[:, cols].astype(jnp.float32) + other[:, cols].astype(jnp.float32)
            ).astype(part.dtype)

    def one_block(rows, put):
        gate = jnp.dot(rows, gate_ref[...], preferred_element_type=jnp.float32)
        up = jnp.dot(rows, up_ref[...], preferred_element_type=jnp.float32)
        hidden_ref[...] = (gate / (1.0 + jnp.exp(-gate)) * up).astype(hidden_ref.dtype)
        step = min(512, width)

        @pl.loop(0, width // step)
        def _(c):
            cols = pl.ds(pl.multiple_of(c * step, step), step)
            put(
                cols,
                jnp.dot(
                    hidden_ref[...], down_ref[:, cols], preferred_element_type=jnp.float32
                ).astype(part.dtype),
            )

    def compute(j):
        if slot_count % 16 == 0:

            def put(cols, val):
                part[j, :, :, cols] = val.reshape(4, slot_count, val.shape[1])

            one_block(slots[j].reshape(4 * slot_count, width), put)
        else:

            @pl.loop(0, 4)
            def _(b):
                def put(cols, val):
                    part[j, b, :, cols] = val

                one_block(slots[j, b], put)

    def inside(j, low):
        return jnp.logical_and(j >= low, j < n)

    @pl.loop(0, n + 5)
    def _(i):
        @pl.when(inside(i, 1))
        def _():
            copy_a(i).wait_recv()
            copy_c(i).start()

        @pl.when(inside(i, near))
        def _():
            copy_y(i).start()

        @pl.when(i == near)
        def _():
            copy_k(near).wait_recv()

            @pl.loop(near + 1, n)
            def _(d):
                copy_f(d).start()

        @pl.when(inside(i - 1, 1))
        def _():
            copy_y(i - 1).wait_recv()
            copy_b(i - 1).start()

        @pl.when(inside(i - 5, 0))
        def _():
            copy_q(i - 5).wait_recv()
            merge((i - 5, own_blk), col_in.at[i - 5])

        @pl.when(inside(i - 3, 0))
        def _():
            copy_p(i - 3).wait_recv()
            for y in range(2):
                merge((i - 3, col * 2 + y), pair_in.at[i - 3, y])

        @pl.when(inside(i - 2, 1))
        def _():
            copy_c(i - 2).wait_recv()
            copy_b(i - 2).wait_recv()

        @pl.when(inside(i - 2, 0))
        def _():
            compute(i - 2)

        @pl.when(inside(i - 5, 1))
        def _():
            copy_r(i - 5).start()

        @pl.when(inside(i - 3, 0))
        def _():
            copy_q(i - 3).start()

        @pl.when(inside(i - 2, 0))
        def _():
            copy_p(i - 2).start()

    def collect(d, rows):
        mix = mix_ref[d]
        high = mix.astype(jnp.bfloat16)
        low = (mix - high.astype(jnp.float32)).astype(jnp.bfloat16)
        both = jnp.dot(high, rows, preferred_element_type=jnp.float32) + jnp.dot(
            low, rows, preferred_element_type=jnp.float32
        )
        return both

    acc[...] = collect(0, part[0, own_blk])

    @pl.loop(1, n)
    def _(d):
        copy_r(d).wait_recv()
        acc[...] += collect(d, back[d])

    @pl.loop(1, near)
    def _(d):
        copy_k(d).wait()

    copy_k(near).wait_send()

    @pl.loop(near + 1, n)
    def _(d):
        copy_f(d).wait()

    keep.wait()
    res_ref[...] = acc[...].astype(res_ref.dtype)

    @pl.loop(1, n)
    def _(d):
        copy_a(d).wait_send()
        copy_y(d).wait_send()
        copy_c(d).wait_send()
        copy_b(d).wait_send()
        copy_r(d).wait_send()

    @pl.loop(0, n)
    def _(d):
        copy_p(d).wait_send()
        copy_q(d).wait_send()


def run_experts(outgoing, nearby, mine, kv, gate_w, up_w, down_w, mix):
    n, capacity, width = outgoing.shape
    hidden_units = gate_w.shape[1]
    tokens = mix.shape[1]
    rows = 4 * capacity if capacity % 16 == 0 else capacity
    dtype = outgoing.dtype
    vmem = pl.BlockSpec(memory_space=pltpu.VMEM)
    flops = 2 * n * 4 * capacity * width * hidden_units * 3
    return pl.pallas_call(
        functools.partial(expert_kernel, n),
        out_shape=(
            jax.ShapeDtypeStruct((tokens, width), dtype),
            jax.ShapeDtypeStruct((n,) + kv.shape, kv.dtype),
        ),
        in_specs=[vmem] * 8,
        out_specs=(vmem, pl.BlockSpec(memory_space=pl.ANY)),
        scratch_shapes=[
            pltpu.VMEM((n, 4, capacity, width), dtype),
            pltpu.VMEM((n, 4, capacity, width), dtype),
            pltpu.VMEM((n, 2, capacity, width), dtype),
            pltpu.VMEM((n, capacity, width), dtype),
            pltpu.VMEM((n, capacity, width), dtype),
            pltpu.VMEM((rows, hidden_units), dtype),
            pltpu.VMEM((tokens, width), jnp.float32),
        ]
        + [pltpu.SemaphoreType.DMA((n,))] * 16
        + [pltpu.SemaphoreType.DMA((5,))],
        compiler_params=pltpu.CompilerParams(
            collective_id=0, has_side_effects=True, vmem_limit_bytes=60 * 1024 * 1024
        ),
        cost_estimate=pl.CostEstimate(
            flops=40 * flops, bytes_accessed=16 * 1024 * 1024, transcendentals=0
        ),
    )(outgoing, nearby, mine, kv, gate_w, up_w, down_w, mix)


def expert_part(kv, moe_rows, moe_gain, routes, route_weights, w_gate, w_up, w_down):
    experts = lax.axis_size("ep")
    tp_count = lax.axis_size("tp")
    me = lax.axis_index("ep")
    tp_id = lax.axis_index("tp")
    dev_rows = moe_rows.shape[0] // tp_count
    top_count = routes.shape[1]
    capacity = max(2, 2 * dev_rows * top_count // experts)
    width = moe_rows.shape[1]
    normed = (
        rms_scaled(moe_rows.astype(jnp.float32), moe_gain)
        .astype(jnp.bfloat16)
        .reshape(tp_count, dev_rows, width)
    )
    relative = jnp.bitwise_xor(routes, me).reshape(tp_count, dev_rows, top_count)
    hits = relative[..., None] == lax.iota(jnp.int32, experts)
    named = jnp.any(hits, axis=2)
    before = (
        lax.iota(jnp.int32, dev_rows)[:, None] > lax.iota(jnp.int32, dev_rows)[None, :]
    ).astype(jnp.bfloat16)
    places = jnp.einsum(
        "ij,bjd->bid", before, named.astype(jnp.bfloat16), preferred_element_type=jnp.float32
    ).astype(jnp.int32)
    places = jnp.where(named, places, -1)
    slot_iota = lax.iota(jnp.int32, capacity)
    take_mine = (places[:, None, :, 0] == slot_iota[None, :, None]).astype(jnp.bfloat16)
    mine = jnp.einsum(
        "bst,btm->bsm", take_mine, normed, preferred_element_type=jnp.float32
    ).astype(jnp.bfloat16)
    own = lambda arr: lax.dynamic_index_in_dim(arr, tp_id, 0, keepdims=False)
    other_id = (1 - tp_id // 2) * 2 + tp_id % 2
    own_places = own(places)

    def fill(block, first, last):
        block_places = lax.dynamic_index_in_dim(places, block, 0, keepdims=False)[:, first:last]
        block_rows = lax.dynamic_index_in_dim(normed, block, 0, keepdims=False)
        take = (block_places.T[:, None, :] == slot_iota[None, :, None]).astype(jnp.bfloat16)
        return (
            jnp.dot(
                take.reshape(-1, dev_rows), block_rows, preferred_element_type=jnp.float32
            )
            .astype(jnp.bfloat16)
            .reshape(last - first, capacity, width)
        )

    outgoing = fill(tp_id, 0, experts)
    nearby = fill(other_id, 0, experts // 2)
    own_weights = own(route_weights.reshape(tp_count, dev_rows, top_count))
    weight_of = jnp.sum(jnp.where(own(hits), own_weights[..., None], 0.0), axis=1)
    mix = jnp.where(
        own_places.T[:, :, None] == slot_iota[None, None, :], weight_of.T[:, :, None], 0.0
    )
    return run_experts(outgoing, nearby, mine, kv, w_gate[0], w_up[0], w_down[0], mix)


def local(
    queries,
    keys,
    values,
    attn_lambda,
    head_gain,
    w_out,
    moe_rows,
    moe_gain,
    routes,
    route_weights,
    w_gate,
    w_up,
    w_down,
):
    positions = queries.shape[0]
    q_heads = queries.shape[1]
    kv_heads = keys.shape[1]
    head_dim = queries.shape[2] // 2
    value_dim = values.shape[2]
    per_key = q_heads // kv_heads
    first_pos = lax.axis_index("ep") * positions
    query_pos = first_pos + lax.iota(jnp.int32, positions)
    last_pos = first_pos + positions - 1
    query_view = queries.reshape(positions, kv_heads, per_key, 2, head_dim)
    inv_scale = head_dim ** (-0.5)
    start_max = jnp.full((positions, kv_heads, per_key, 2), MASKED, jnp.float32)
    start_total = jnp.zeros((positions, kv_heads, per_key, 2), jnp.float32)
    start_acc = jnp.zeros((positions, kv_heads, per_key, 2, value_dim), jnp.float32)
    carry = (start_max, start_total, start_acc)
    both = jnp.concatenate([keys, values], axis=2)
    moe_out, gathered = expert_part(
        both.reshape(positions, -1),
        moe_rows,
        moe_gain,
        routes,
        route_weights,
        w_gate,
        w_up,
        w_down,
    )
    gathered = gathered.reshape(-1, kv_heads, both.shape[2])
    key_piece = gathered[:, :, : keys.shape[2]]
    value_piece = gathered[:, :, keys.shape[2] :]
    shard_count = key_piece.shape[0] // positions
    together = 1
    for candidate in (2, 3, 4):
        if shard_count % candidate == 0:
            together = candidate
    block_len = together * positions
    blocks = shard_count // together
    key_blocks = key_piece.reshape(blocks, block_len, kv_heads, 2, head_dim)
    value_blocks = value_piece.reshape(blocks, block_len, kv_heads, value_dim)
    block_starts = block_len * lax.iota(jnp.int32, blocks)

    def visit(running, inputs):
        key_blk, value_blk, block_start = inputs

        def update(current):
            run_max, run_total, run_acc = current
            key_pos = block_start + lax.iota(jnp.int32, block_len)
            scores = (
                jnp.einsum(
                    "qkgmd,pkmd->qkgmp", query_view, key_blk, preferred_element_type=jnp.float32
                )
                * inv_scale
            )
            allowed = key_pos[None, :] <= query_pos[:, None]
            scores = jnp.where(allowed[:, None, None, None, :], scores, MASKED)
            new_max = jnp.maximum(run_max, jnp.max(scores, axis=-1))
            shrink = jnp.exp(run_max - new_max)
            weights = jnp.exp(scores - new_max[..., None])
            run_total = run_total * shrink + jnp.sum(weights, axis=-1)
            run_acc = run_acc * shrink[..., None] + jnp.einsum(
                "qkgmp,pkv->qkgmv",
                weights.astype(jnp.bfloat16),
                value_blk,
                preferred_element_type=jnp.float32,
            )
            return (new_max, run_total, run_acc)

        def keep(current):
            return current

        return (lax.cond(block_start <= last_pos, update, keep, running), None)

    carry, unused = lax.scan(visit, carry, (key_blocks, value_blocks, block_starts))
    run_max, run_total, run_acc = carry
    ratios = run_acc / run_total[..., None]
    lambda_view = attn_lambda.reshape(1, kv_heads, per_key, 1)
    head_out = ratios[:, :, :, 0] - lambda_view * ratios[:, :, :, 1]
    attn_rows = (
        rms_scaled(head_out, head_gain).astype(jnp.bfloat16).reshape(positions, q_heads * value_dim)
    )
    tp_count = lax.axis_size("tp")
    tp_id = lax.axis_index("tp")
    exchanged = lax.all_to_all(
        attn_rows.reshape(positions, q_heads, value_dim),
        "tp",
        split_axis=0,
        concat_axis=1,
        tiled=True,
    )
    mixer_out = jnp.dot(
        exchanged.reshape(positions // tp_count, tp_count * q_heads * value_dim),
        w_out,
        preferred_element_type=jnp.float32,
    ).astype(jnp.bfloat16)
    return (mixer_out, moe_out)


def solution(mesh):
    return jax.shard_map(
        local,
        mesh=mesh,
        in_specs=(
            P("ep", "tp", None),
            P("ep", "tp", None),
            P("ep", "tp", None),
            P("tp"),
            P(),
            P(),
            P("ep", None),
            P(),
            P("ep", None),
            P("ep", None),
            P("ep", None, "tp"),
            P("ep", None, "tp"),
            P("ep", "tp", None),
        ),
        out_specs=(P(("ep", "tp"), None), P(("ep", "tp"), None)),
        check_vma=False,
    )
```

profile of v0, /device:TPU:16, one launch (start us, length us, event | category | flops | bytes accessed | tf_op | source)
XLA Modules:
  0.0 194.8 jit_solution(17685315207769105349)
XLA Ops:
  1.2 0.7 xor_bitcast_fusion
  2.1 2.1 %fusion.23 = f32[512]{0:T(512)S(1)} fusion(bf16[512,2048]{1,0:T(8,128)(2,1)} %param.23), kind=kLoop, calls=%fused_computation.28 | loop fusion | flops 3145216 | bytes 2099200 | tf_op jit(solution)/shard_map/reduce_sum | solution.py:15
  4.3 2.1 %fusion.25 = bf16[512,2048]{1,0:T(8,128)(2,1)S(1)} fusion(bf16[512,2048]{1,0:T(8,128)(2,1)} %param.23, f32[2048]{0:T(1024)} %param.24, f32[512]{0:T(512)S(1)} %add_rsqrt_fusion.1), kind=kLoop, calls=%fused_computation.30 | loop fusion | flops 4194304 | bytes 4204544 | tf_op jit(solution)/shard_map/convert_element_type | solution.py:368
  6.4 2.0 %convolution_convert_fusion = bf16[512,2048]{1,0:T(8,128)(2,1)} fusion(pred[512,128]{1,0:T(32,128)(4,1)S(1)} %bitcast.142, bf16[4,128,2048]{2,1,0:T(8,128)(2,1)S(1)} %bitcast.132, s32[]{:T(128)S(6)} %select_n.45), kind=kOutput, calls=%fused_computation.31 | convolution fusion | flops 269484032 | bytes 2686980 | tf_op jit(solution)/shard_map/dot_general | solution.py:395
  8.5 1.4 convolution_convert_fusion.2
  9.9 1.1 fusion.32.mix_ref
  11.0 1.4 convolution_convert_fusion.1.mine_ref
  12.4 0.7 maximum_bitcast_fusion.kv_ref
  13.1 154.1 %shard_map.140 = (bf16[128,2048]{1,0:T(8,128)(2,1)}, bf16[8,256,256]{2,1,0:T(8,128)(2,1)}) custom-call(bf16[8,64,2048]{2,1,0:T(8,128)(2,1)} %bitcast.135, bf16[4,64,2048]{2,1,0:T(8,128)(2,1)} %bitcast.138, bf16[4,64,2048]{2,1,0:T(8,128)(2,1)} %convolution_convert_fusion.1.mine_ref, bf16[256,256]{1,0:T(8,128)(2,1)} %maximum_bitcast_fusion.kv_ref, ...), custom_call_target="tpu_custom_call" | custom-call | flops 257698037760 | bytes 16777216 | tf_op jit(solution)/shard_map/pallas_call | solution.py:329
  167.3 1.3 fusion.47
  169.0 0.7 copy.79
  170.2 9.3 %while.15 = (s32[]{:T(128)}, f32[256,1,2,2]{0,2,3,1:T(2,128)S(1)}, f32[256,1,2,2]{0,2,3,1:T(2,128)S(1)}, f32[256,1,2,2,128]{0,4,3,2,1:T(8,128)S(1)}, s32[2]{0:T(...) while((s32[]{:T(128)}, f32[256,1,2,2]{0,2,3,1:T(2,128)S(1)}, ...), condition=%wide.region_8.9_spmd.clone, body=%wide.region_3.8_spmd.clone.sunk | while | flops 411570432 | bytes 15155487 | solution.py:498
  171.5 3.4 %conditional.3 = ((f32[256,1,2,2]{0,2,3,1:T(2,128)S(1)}, f32[256,1,2,2]{0,2,3,1:T(2,128)S(1)}, f32[256,1,2,2,128]{0,4,3,2,1:T(8,128)S(1)})) conditional(s32[]{:T(128)} %convert_element_type.76, (f32[256,1,2,2]{0,2,3,1:T(2,128)S(1)}, f32[256,1,2,2]{0,2,3,1:T(2,128)S(1)}, f32[256,1,2,2,128]{0,4,3,2,1:T(8,128)S(1)}) %tuple.51, (s32[]{:T(128)}, ...), branch_computations={%region_4.4_spmd, %region_5.7_spmd} | conditional | flops 411570432 | bytes 15154224 | solution.py:496
  172.4 0.9 fusion.4
  173.3 1.0 fusion.5
  176.1 3.4 %conditional.3 = ((f32[256,1,2,2]{0,2,3,1:T(2,128)S(1)}, f32[256,1,2,2]{0,2,3,1:T(2,128)S(1)}, f32[256,1,2,2,128]{0,4,3,2,1:T(8,128)S(1)})) conditional(s32[]{:T(128)} %convert_element_type.76, (f32[256,1,2,2]{0,2,3,1:T(2,128)S(1)}, f32[256,1,2,2]{0,2,3,1:T(2,128)S(1)}, f32[256,1,2,2,128]{0,4,3,2,1:T(8,128)S(1)}) %tuple.51, (s32[]{:T(128)}, ...), branch_computations={%region_4.4_spmd, %region_5.7_spmd} | conditional | flops 411570432 | bytes 15154224 | solution.py:496
  177.0 0.9 fusion.4
  177.9 1.0 fusion.5
  179.9 0.7 broadcast_divide_fusion
  181.1 1.0 fusion.39
  182.1 3.3 %all-to-all-start = ((bf16[256,2,128]{2,1,0:T(2,128)(2,1)}), bf16[256,2,128]{2,1,0:T(2,128)(2,1)S(1)}, u32[]{:S(2)}, u32[]{:S(2)}) async-start(bf16[256,2,128]{2,1,0:T(2,128)(2,1)} %fusion.39), calls=%async_computation | async-start | bytes 262144 | tf_op jit(solution)/shard_map/all_to_all | solution.py:508
  185.5 4.6 %all-to-all-done = bf16[256,2,128]{2,1,0:T(2,128)(2,1)S(1)} async-done(((bf16[256,2,128]{2,1,0:T(2,128)(2,1)}), bf16[256,2,128]{2,1,0:T(2,128)(2,1)S(1)}, u32[]{:S(2)}, u32[]{:S(2)}) %all-to-all-start) | async-done | bytes 131104 | tf_op jit(solution)/shard_map/all_to_all | solution.py:508
  190.3 3.7 %convolution_convert_fusion.3 = bf16[64,2048]{1,0:T(8,128)(2,1)} fusion(bf16[64,1024]{1,0:T(8,128)(2,1)S(1)} %reshape.264, bf16[1024,2048]{1,0:T(8,128)(2,1)} %param.22), kind=kOutput, calls=%fused_computation.34 | convolution fusion | flops 268566528 | bytes 4587520 | tf_op jit(solution)/shard_map/dot_general | solution.py:515
  194.0 0.8 copy.126
  (61 shorter events, 6.7 us)
Async XLA Ops:
  0.6 9.3 %copy-start = (f32[512,2]{0,1:T(2,128)S(1)}, f32[512,2]{0,1:T(2,128)}, u32[]{:S(2)}) copy-start(f32[512,2]{0,1:T(2,128)} %param.26) | copy-start | bytes 12292
  6.4 6.0 %copy-start.3 = (bf16[256,1,128]{2,0,1:T(8,128)(2,1)S(1)}, bf16[256,1,128]{2,0,1:T(8,128)(2,1)}, u32[]{:S(2)}) copy-start(bf16[256,1,128]{2,0,1:T(8,128)(2,1)} %param.19) | copy-start | bytes 196612
  6.4 6.0 %copy-start.4 = (bf16[256,1,128]{2,0,1:T(8,128)(2,1)S(1)}, bf16[256,1,128]{2,0,1:T(8,128)(2,1)}, u32[]{:S(2)}) copy-start(bf16[256,1,128]{2,0,1:T(8,128)(2,1)} %param.18) | copy-start | bytes 196612
  167.3 2.7 %copy-start.2 = (bf16[256,2,128]{2,1,0:T(2,128)(2,1)S(1)}, bf16[256,2,128]{2,1,0:T(2,128)(2,1)}, u32[]{:S(2)}) copy-start(bf16[256,2,128]{2,1,0:T(2,128)(2,1)} %param.17) | copy-start | bytes 393220
  167.3 2.9 %copy-start.7 = (s32[2]{0:T(128)S(1)}, s32[2]{0:T(128)}, u32[]{:S(2)}) copy-start(s32[2]{0:T(128)} %iota_multiply_fusion) | copy-start | bytes 28
  170.2 10.4 %copy-start.5 = (f32[2]{0:T(128)S(1)}, f32[2]{0:T(128)}, u32[]{:S(2)}) copy-start(f32[2]{0:T(128)} %param.20) | copy-start | bytes 28
  170.2 10.9 %copy-start.6 = (f32[128]{0:T(128)S(1)}, f32[128]{0:T(128)}, u32[]{:S(2)}) copy-start(f32[128]{0:T(128)} %param.21) | copy-start | bytes 1540
  179.9 14.1 %copy-start.1 = (bf16[128,2048]{1,0:T(8,128)(2,1)S(1)}, bf16[128,2048]{1,0:T(8,128)(2,1)}, u32[]{:S(2)}) copy-start(bf16[128,2048]{1,0:T(8,128)(2,1)} %get-tuple-element.364) | copy-start | bytes 1572868
  182.1 7.9 %all-to-all-start = ((bf16[256,2,128]{2,1,0:T(2,128)(2,1)}), bf16[256,2,128]{2,1,0:T(2,128)(2,1)S(1)}, u32[]{:S(2)}, u32[]{:S(2)}) async-start(bf16[256,2,128]{2,1,0:T(2,128)(2,1)} %fusion.39), calls=%async_computation | async-start | bytes 262144 | tf_op jit(solution)/shard_map/all_to_all | solution.py:508
where the time goes:
time: 195 us
  Pallas kernels  154 us (79%)
  other arithmetic  13.3 us (7%)
  matrix products  11.6 us (6%)
  local copies, waits for them, and re-layouts  5.56 us (3%)
  waiting for transfers between devices  4.57 us (2%)
  starting transfers between devices  3.33 us (2%)
    pallas_call x1, Pallas kernels, run_experts(): pl.pallas_call(functools.partial(expert_kernel, n), out_shape=(jax.ShapeD...  154 us
    all_to_all x1, waiting for transfers between devices, local(): lax.all_to_all(attn_rows.reshape(positions, q_heads, value_dim), 'tp', sp...  4.57 us
  transfers between devices with their start and end apart: 1, of which 1 were waited for; matrix products, arithmetic and copies ran while one was open for 0% of the time, Pallas kernels for 0%

commit v1 on v0

--- a/solution.py
+++ b/solution.py
@@ -407,6 +407,621 @@
         own_places.T[:, :, None] == slot_iota[None, None, :], weight_of.T[:, :, None], 0.0
     )
     return run_experts(outgoing, nearby, mine, kv, w_gate[0], w_up[0], w_down[0], mix)
+
+
+def layer_kernel(
+    n,
+    rows_ref,
+    gain_ref,
+    places_ref,
+    place_cols_ref,
+    weight_cols_ref,
+    q_ref,
+    kv_ref,
+    lam_ref,
+    head_gain_ref,
+    gate_hbm,
+    up_hbm,
+    down_hbm,
+    w_out_hbm,
+    mixer_ref,
+    res_ref,
+    gate_ref,
+    up_ref,
+    down_ref,
+    w_out_ref,
+    normed,
+    packs,
+    near_packs,
+    kv_all,
+    slots,
+    part,
+    pair_in,
+    col_in,
+    back,
+    hidden_ref,
+    acc,
+    run_max,
+    run_total,
+    run_acc,
+    attn,
+    heads_all,
+    send_k,
+    recv_k,
+    send_a,
+    recv_a,
+    send_y,
+    recv_y,
+    send_c,
+    recv_c,
+    send_b,
+    recv_b,
+    send_p,
+    recv_p,
+    send_q,
+    recv_q,
+    send_r,
+    recv_r,
+    send_h,
+    recv_h,
+    local_sem,
+):
+    me = lax.axis_index("ep")
+    tp = lax.axis_index("tp")
+    row = tp // 2
+    col = tp % 2
+    other_row = 1 - row
+    other_col = 1 - col
+    pair_peer = row * 2 + other_col
+    row_peer = other_row * 2 + col
+    own_blk = col * 2 + row
+    far_blk = col * 2 + other_row
+    slot_count = slots.shape[2]
+    width = slots.shape[3]
+    dev_rows = rows_ref.shape[1]
+    step = min(512, width)
+    near = n // 2
+    bits = [1 << b for b in range(n.bit_length() - 1)]
+
+    def partner(d):
+        total = 0
+        for bit in bits:
+            total = total + (me // bit + d // bit) % 2 * bit
+        return total
+
+    def remote(src, dst, ssem, rsem, ep_id, tp_id):
+        return pltpu.make_async_remote_copy(
+            src_ref=src,
+            dst_ref=dst,
+            send_sem=ssem,
+            recv_sem=rsem,
+            device_id=(ep_id, tp_id),
+            device_id_type=pl.DeviceIdType.MESH,
+        )
+
+    loads = [
+        pltpu.make_async_copy(src, dst, local_sem.at[i])
+        for i, (src, dst) in enumerate(
+            (
+                (gate_hbm, gate_ref),
+                (up_hbm, up_ref),
+                (down_hbm, down_ref),
+                (kv_ref, kv_all.at[me]),
+                (w_out_hbm, w_out_ref),
+            )
+        )
+    ]
+    for load in loads:
+        load.start()
+
+    barrier = pltpu.get_barrier_semaphore()
+
+    @pl.loop(1, n)
+    def _(d):
+        pl.semaphore_signal(
+            barrier, inc=1, device_id=(partner(d), tp), device_id_type=pl.DeviceIdType.MESH
+        )
+
+    @pl.loop(1, 4)
+    def _(t):
+        pl.semaphore_signal(
+            barrier, inc=1, device_id=(me, (tp + t) % 4), device_id_type=pl.DeviceIdType.MESH
+        )
+
+    def norm_block(b):
+        @pl.loop(0, dev_rows // 16)
+        def _(r):
+            piece = pl.ds(pl.multiple_of(r * 16, 16), 16)
+            normed[b, piece, :] = rms_scaled(
+                rows_ref[b, piece, :].astype(jnp.float32), gain_ref[...]
+            ).astype(normed.dtype)
+
+    slot_iota = lax.broadcasted_iota(jnp.int32, (slot_count, dev_rows), 0)
+
+    def take(b, first, last):
+        places = places_ref[b]
+        return jnp.concatenate(
+            [
+                jnp.where(places[d : d + 1, :] == slot_iota, 1.0, 0.0)
+                for d in range(first, last)
+            ],
+            axis=0,
+        ).astype(jnp.bfloat16)
+
+    def select(b, taken, put):
+        @pl.loop(0, width // step)
+        def _(c):
+            cols = pl.ds(pl.multiple_of(c * step, step), step)
+            put(
+                cols,
+                jnp.dot(
+                    taken, normed[b, :, cols], preferred_element_type=jnp.float32
+                ).astype(packs.dtype),
+            )
+
+    def copy_a(d):
+        return remote(
+            packs.at[d], slots.at[d, own_blk], send_a.at[d], recv_a.at[d], partner(d), tp
+        )
+
+    def copy_k(d):
+        return remote(kv_ref, kv_all.at[me], send_k.at[d], recv_k.at[d], partner(d), tp)
+
+    def copy_f(d):
+        block = kv_all.at[partner(near)]
+        return remote(block, block, send_k.at[d], recv_k.at[d], partner(d - near), tp)
+
+    def copy_n(d):
+        return remote(
+            near_packs.at[d], slots.at[d, far_blk], send_y.at[d], recv_y.at[d], partner(d), tp
+        )
+
+    def copy_y(d):
+        block = slots.at[d, own_blk]
+        return remote(block, block, send_y.at[d], recv_y.at[d], me, row_peer)
+
+    def copy_c(d):
+        block = slots.at[d, own_blk]
+        return remote(block, block, send_c.at[d], recv_c.at[d], me, pair_peer)
+
+    def copy_b(d):
+        block = slots.at[d, far_blk]
+        return remote(block, block, send_b.at[d], recv_b.at[d], me, pair_peer)
+
+    def copy_p(d):
+        return remote(
+            part.at[d, pl.ds(other_col * 2, 2)],
+            pair_in.at[d],
+            send_p.at[d],
+            recv_p.at[d],
+            me,
+            pair_peer,
+        )
+
+    def copy_q(d):
+        return remote(part.at[d, far_blk], col_in.at[d], send_q.at[d], recv_q.at[d], me, row_peer)
+
+    def copy_r(d):
+        return remote(
+            part.at[d, own_blk], back.at[d], send_r.at[d], recv_r.at[d], partner(d), tp
+        )
+
+    positions = kv_ref.shape[0]
+    piece_rows = positions // 4
+
+    def copy_h(t):
+        peer = (tp + t) % 4
+        return remote(
+            attn.at[pl.ds(pl.multiple_of(peer * piece_rows, piece_rows), piece_rows)],
+            heads_all.at[tp],
+            send_h.at[t],
+            recv_h.at[t],
+            me,
+            peer,
+        )
+
+    norm_block(tp)
+
+    def put_far(cols, val):
+        packs[near:n, :, cols] = val.reshape(n - near, slot_count, val.shape[1])
+
+    select(tp, take(tp, near, n), put_far)
+    pl.semaphore_wait(barrier, n + 2)
+
+    @pl.loop(near, n)
+    def _(d):
+        copy_a(d).start()
+
+    loads[3].wait()
+    low = me < near
+
+    @pl.when(low)
+    def _():
+        copy_k(near).start()
+
+    def put_near(cols, val):
+        packs[0:near, :, cols] = val.reshape(near, slot_count, val.shape[1])
+
+    select(tp, take(tp, 0, near), put_near)
+
+    @pl.loop(1, near)
+    def _(d):
+        copy_a(d).start()
+
+    norm_block(row_peer)
+
+    def put_other(cols, val):
+        near_packs[:, :, cols] = val.reshape(near, slot_count, val.shape[1])
+
+    select(row_peer, take(row_peer, 0, near), put_other)
+
+    @pl.loop(1, near)
+    def _(d):
+        copy_n(d).start()
+
+        @pl.when(partner(d) > me)
+        def _():
+            copy_k(d).start()
+
+    fills = [
+        pltpu.make_async_copy(packs.at[0], slots.at[0, own_blk], local_sem.at[5]),
+        pltpu.make_async_copy(near_packs.at[0], slots.at[0, far_blk], local_sem.at[6]),
+    ]
+    for fill in fills:
+        fill.start()
+
+    for peer_row in range(2):
+        block = peer_row * 2 + other_col
+        norm_block(block)
+
+        def put_mine(cols, val, peer_row=peer_row):
+            slots[0, other_col * 2 + peer_row, :, cols] = val
+
+        select(block, take(block, 0, 1), put_mine)
+    for fill in fills:
+        fill.wait()
+    for load in loads[:3]:
+        load.wait()
+
+    def merge(index, other):
+        rows = part.at[index]
+
+        @pl.loop(0, width // step)
+        def _(c):
+            cols = pl.ds(pl.multiple_of(c * step, step), step)
+            rows[:, cols] = (
+                rows[:, cols].astype(jnp.float32) + other[:, cols].astype(jnp.float32)
+            ).astype(part.dtype)
+
+    def compute(j):
+        rows = slots[j].reshape(4 * slot_count, width)
+        gate = jnp.dot(rows, gate_ref[...], preferred_element_type=jnp.float32)
+        up = jnp.dot(rows, up_ref[...], preferred_element_type=jnp.float32)
+        hidden_ref[...] = (gate / (1.0 + jnp.exp(-gate)) * up).astype(hidden_ref.dtype)
+
+        @pl.loop(0, width // step)
+        def _(c):
+            cols = pl.ds(pl.multiple_of(c * step, step), step)
+            val = jnp.dot(
+                hidden_ref[...], down_ref[:, cols], preferred_element_type=jnp.float32
+            ).astype(part.dtype)
+            part[j, :, :, cols] = val.reshape(4, slot_count, step)
+
+    def order(i):
+        far_step = near + i - 1
+        return jnp.where(i <= 0, 0, jnp.where(i <= near, far_step, i - near))
+
+    def inside(j, low_bound):
+        return jnp.logical_and(j >= low_bound, j < n)
+
+    @pl.loop(0, n + 2)
+    def _(i):
+        d_in = order(i)
+        d_mid = order(i - 1)
+        d_out = order(i - 2)
+
+        @pl.when(inside(i, 1))
+        def _():
+            copy_a(d_in).wait_recv()
+            copy_c(d_in).start()
+
+            @pl.when(d_in >= near)
+            def _():
+                copy_y(d_in).start()
+
+        @pl.when(inside(i - 1, 1))
+        def _():
+            copy_y(d_mid).wait_recv()
+            copy_b(d_mid).start()
+            copy_c(d_mid).wait_recv()
+            copy_b(d_mid).wait_recv()
+
+        @pl.when(inside(i - 1, 0))
+        def _():
+            compute(d_mid)
+            copy_p(d_mid).start()
+
+        @pl.when(inside(i - 2, 0))
+        def _():
+            copy_q(d_out).wait_recv()
+            merge((d_out, own_blk), col_in.at[d_out])
+
+        @pl.when(inside(i - 2, 1))
+        def _():
+            copy_r(d_out).start()
+
+        @pl.when(inside(i - 1, 0))
+        def _():
+            copy_p(d_mid).wait_recv()
+            for y in range(2):
+                merge((d_mid, col * 2 + y), pair_in.at[d_mid, y])
+            copy_q(d_mid).start()
+
+        @pl.when(jnp.logical_and(i == near + 1, jnp.logical_not(low)))
+        def _():
+            copy_k(near).wait_recv()
+
+            @pl.loop(near + 1, n)
+            def _(d):
+                copy_f(d).start()
+
+    @pl.loop(1, near)
+    def _(d):
+        @pl.when(partner(d) < me)
+        def _():
+            copy_k(d).wait_recv()
+
+    @pl.when(jnp.logical_not(low))
+    def _():
+        @pl.loop(near + 1, n)
+        def _(d):
+            copy_f(d).wait_recv()
+
+    head_dim2 = kv_ref.shape[1] // 2
+    q_heads = q_ref.shape[1] // head_dim2
+    inv_scale = (head_dim2 // 2) ** (-0.5)
+    run_max[...] = jnp.full(run_max.shape, MASKED, jnp.float32)
+    run_total[...] = jnp.zeros(run_total.shape, jnp.float32)
+    run_acc[...] = jnp.zeros(run_acc.shape, jnp.float32)
+    map_of = lax.broadcasted_iota(jnp.int32, (positions, head_dim2), 1) // (head_dim2 // 2)
+
+    @pl.loop(0, me + 1)
+    def _(kb):
+        keys = kv_all[kb, :, :head_dim2]
+        vals = kv_all[kb, :, head_dim2:]
+        gap = (me - kb) * positions
+        allowed = (
+            lax.broadcasted_iota(jnp.int32, (positions, positions), 1)
+            <= lax.broadcasted_iota(jnp.int32, (positions, positions), 0) + gap
+        )
+        for h in range(q_heads):
+            for m in range(2):
+                at = h * 2 + m
+                query = q_ref[:, h * head_dim2 : (h + 1) * head_dim2]
+                query = jnp.where(map_of == m, query, jnp.zeros_like(query))
+                scores = (
+                    lax.dot_general(
+                        query, keys, (((1,), (1,)), ((), ())), preferred_element_type=jnp.float32
+                    )
+                    * inv_scale
+                )
+                scores = jnp.where(allowed, scores, MASKED)
+                old_max = run_max[at]
+                new_max = jnp.maximum(old_max, jnp.max(scores, axis=1, keepdims=True))
+                shrink = jnp.exp(old_max - new_max)
+                weights = jnp.exp(scores - new_max)
+                run_max[at] = new_max
+                run_total[at] = run_total[at] * shrink + jnp.sum(weights, axis=1, keepdims=True)
+                run_acc[at] = run_acc[at] * shrink + jnp.dot(
+                    weights.astype(jnp.bfloat16), vals, preferred_element_type=jnp.float32
+                )
+
+    for h in range(q_heads):
+        head_out = (
+            run_acc[2 * h] / run_total[2 * h]
+            - lam_ref[h] * run_acc[2 * h + 1] / run_total[2 * h + 1]
+        )
+        attn[:, h * head_dim2 : (h + 1) * head_dim2] = rms_scaled(
+            head_out, head_gain_ref[...]
+        ).astype(attn.dtype)
+
+    for t in range(1, 4):
+        copy_h(t).start()
+    heads_all[tp] = attn[pl.ds(pl.multiple_of(tp * piece_rows, piece_rows), piece_rows), :]
+
+    def collect(d, rows):
+        lanes = lax.broadcasted_iota(jnp.int32, place_cols_ref.shape, 1)
+        place = jnp.sum(jnp.where(lanes == d, place_cols_ref[...], 0), axis=1, keepdims=True)
+        weight = jnp.sum(jnp.where(lanes == d, weight_cols_ref[...], 0.0), axis=1, keepdims=True)
+        slot = lax.broadcasted_iota(jnp.int32, (dev_rows, slot_count), 1)
+        mix = jnp.where(slot == place, weight, 0.0)
+        high = mix.astype(jnp.bfloat16)
+        low_part = (mix - high.astype(jnp.float32)).astype(jnp.bfloat16)
+
+        @pl.loop(0, width // step)
+        def _(c):
+            cols = pl.ds(pl.multiple_of(c * step, step), step)
+            piece = rows[:, cols]
+            acc[:, cols] += jnp.dot(high, piece, preferred_element_type=jnp.float32) + jnp.dot(
+                low_part, piece, preferred_element_type=jnp.float32
+            )
+
+    acc[...] = jnp.zeros(acc.shape, jnp.float32)
+    collect(0, part.at[0, own_blk])
+
+    @pl.loop(1, near)
+    def _(d):
+        copy_r(d).wait_recv()
+        collect(d, back.at[d])
+
+    loads[4].wait()
+    for t in range(1, 4):
+        copy_h(t).wait_recv()
+    mixed = heads_all.shape[2]
+
+    @pl.loop(0, width // step)
+    def _(c):
+        cols = pl.ds(pl.multiple_of(c * step, step), step)
+        total = jnp.zeros((piece_rows, step), jnp.float32)
+        for t in range(4):
+            total = total + jnp.dot(
+                heads_all[t],
+                w_out_ref[t * mixed : (t + 1) * mixed, cols],
+                preferred_element_type=jnp.float32,
+            )
+        mixer_ref[:, cols] = total.astype(mixer_ref.dtype)
+
+    @pl.loop(near, n)
+    def _(d):
+        copy_r(d).wait_recv()
+        collect(d, back.at[d])
+
+    res_ref[...] = acc[...].astype(res_ref.dtype)
+
+    @pl.when(low)
+    def _():
+        copy_k(near).wait_send()
+
+    @pl.loop(1, near)
+    def _(d):
+        copy_n(d).wait_send()
+
+        @pl.when(partner(d) > me)
+        def _():
+            copy_k(d).wait_send()
+
+    @pl.when(jnp.logical_not(low))
+    def _():
+        @pl.loop(near + 1, n)
+        def _(d):
+            copy_f(d).wait_send()
+
+    @pl.loop(near, n)
+    def _(d):
+        copy_y(d).wait_send()
+
+    @pl.loop(1, n)
+    def _(d):
+        copy_a(d).wait_send()
+        copy_c(d).wait_send()
+        copy_b(d).wait_send()
+        copy_r(d).wait_send()
+
+    @pl.loop(0, n)
+    def _(d):
+        copy_p(d).wait_send()
+        copy_q(d).wait_send()
+
+    for t in range(1, 4):
+        copy_h(t).wait_send()
+
+
+def run_layer(n, capacity, rows, gain, places, place_cols, weight_cols, q, kv, lam, head_gain, mats):
+    tp_count, dev_rows, width = rows.shape
+    gate_w, up_w, down_w, w_out = mats
+    hidden_units = gate_w.shape[1]
+    positions, mixed = q.shape
+    head_dim2 = kv.shape[1] // 2
+    maps = 2 * mixed // head_dim2
+    dtype = rows.dtype
+    near = n // 2
+    vmem = pl.BlockSpec(memory_space=pltpu.VMEM)
+    hbm = pl.BlockSpec(memory_space=pl.ANY)
+    flops = 2 * n * 4 * capacity * width * hidden_units * 3
+    return pl.pallas_call(
+        functools.partial(layer_kernel, n),
+        out_shape=(
+            jax.ShapeDtypeStruct((positions // tp_count, width), dtype),
+            jax.ShapeDtypeStruct((dev_rows, width), dtype),
+        ),
+        in_specs=[vmem] * 7 + [pl.BlockSpec(memory_space=pltpu.SMEM), vmem] + [hbm] * 4,
+        out_specs=(vmem, vmem),
+        scratch_shapes=[
+            pltpu.VMEM(gate_w.shape, dtype),
+            pltpu.VMEM(up_w.shape, dtype),
+            pltpu.VMEM(down_w.shape, dtype),
+            pltpu.VMEM(w_out.shape, dtype),
+            pltpu.VMEM((tp_count, dev_rows, width), dtype),
+            pltpu.VMEM((n, capacity, width), dtype),
+            pltpu.VMEM((near, capacity, width), dtype),
+            pltpu.VMEM((n,) + kv.shape, dtype),
+            pltpu.VMEM((n, 4, capacity, width), dtype),
+            pltpu.VMEM((n, 4, capacity, width), dtype),
+            pltpu.VMEM((n, 2, capacity, width), dtype),
+            pltpu.VMEM((n, capacity, width), dtype),
+            pltpu.VMEM((n, capacity, width), dtype),
+            pltpu.VMEM((4 * capacity, hidden_units), dtype),
+            pltpu.VMEM((dev_rows, width), jnp.float32),
+            pltpu.VMEM((maps, positions, 1), jnp.float32),
+            pltpu.VMEM((maps, positions, 1), jnp.float32),
+            pltpu.VMEM((maps, positions, head_dim2), jnp.float32),
+            pltpu.VMEM((positions, mixed), dtype),
+            pltpu.VMEM((tp_count, positions // tp_count, mixed), dtype),
+        ]
+        + [pltpu.SemaphoreType.DMA((n,))] * 16
+        + [pltpu.SemaphoreType.DMA((4,))] * 2
+        + [pltpu.SemaphoreType.DMA((7,))],
+        compiler_params=pltpu.CompilerParams(
+            collective_id=1, has_side_effects=True, vmem_limit_bytes=60 * 1024 * 1024
+        ),
+        cost_estimate=pl.CostEstimate(
+            flops=40 * flops, bytes_accessed=16 * 1024 * 1024, transcendentals=0
+        ),
+    )(rows, gain, places, place_cols, weight_cols, q, kv, lam, head_gain, *mats)
+
+
+def one_kernel(
+    queries,
+    keys,
+    values,
+    attn_lambda,
+    head_gain,
+    w_out,
+    moe_rows,
+    moe_gain,
+    routes,
+    route_weights,
+    w_gate,
+    w_up,
+    w_down,
+):
+    experts = lax.axis_size("ep")
+    tp_count = lax.axis_size("tp")
+    me = lax.axis_index("ep")
+    tp_id = lax.axis_index("tp")
+    positions = queries.shape[0]
+    width = moe_rows.shape[1]
+    dev_rows = moe_rows.shape[0] // tp_count
+    top_count = routes.shape[1]
+    capacity = 2 * dev_rows * top_count // experts
+    relative = jnp.bitwise_xor(routes, me).reshape(tp_count, dev_rows, top_count)
+    hits = relative[..., None] == lax.iota(jnp.int32, experts)
+    named = jnp.any(hits, axis=2)
+    before = (
+        lax.iota(jnp.int32, dev_rows)[:, None] > lax.iota(jnp.int32, dev_rows)[None, :]
+    ).astype(jnp.bfloat16)
+    places = jnp.einsum(
+        "ij,bjd->bid", before, named.astype(jnp.bfloat16), preferred_element_type=jnp.float32
+    ).astype(jnp.int32)
+    places = jnp.where(named, places, -1)
+    own = lambda arr: lax.dynamic_index_in_dim(arr, tp_id, 0, keepdims=False)
+    own_weights = own(route_weights.reshape(tp_count, dev_rows, top_count))
+    weight_cols = jnp.sum(jnp.where(own(hits), own_weights[..., None], 0.0), axis=1)
+    kv = jnp.concatenate([keys, values], axis=2).reshape(positions, -1)
+    return run_layer(
+        experts,
+        capacity,
+        moe_rows.reshape(tp_count, dev_rows, width),
+        moe_gain.reshape(1, width),
+        jnp.transpose(places, (0, 2, 1)),
+        own(places),
+        weight_cols,
+        queries.reshape(positions, -1),
+        kv,
+        attn_lambda,
+        head_gain.reshape(1, -1),
+        (w_gate[0], w_up[0], w_down[0], w_out),
+    )
 
 
 def local(
@@ -521,8 +1136,16 @@
 
 
 def solution(mesh):
+    experts, tp_count = mesh.shape["ep"], mesh.shape["tp"]
+
+    def body(*args):
+        keys, moe_rows, routes = args[1], args[6], args[8]
+        capacity = 2 * (moe_rows.shape[0] // tp_count) * routes.shape[1] // experts
+        whole_tiles = capacity % 16 == 0 and keys.shape[1] == 1
+        return (one_kernel if whole_tiles else local)(*args)
+
     return jax.shard_map(
-        local,
+        body,
         mesh=mesh,
         in_specs=(
             P("ep", "tp", None),

time: 195 us -> 154 us (0.79)
  the two profiles are of different devices: /device:TPU:16 before, /device:TPU:27 now
where the time goes in v1:
time: 154 us; the launch traced here: 152 us
  Pallas kernels  141 us (92%)
  local copies, waits for them, and re-layouts  7.24 us (5%)
  other arithmetic  2.26 us (1%)
    pallas_call x1, Pallas kernels, run_layer(): pl.pallas_call(functools.partial(layer_kernel, n), out_shape=(jax.ShapeDt...  141 us
    unnamed x5, local copies, waits for them, and re-layouts  5.81 us

profile of v1, /device:TPU:27, one launch (start us, length us, event | category | flops | bytes accessed | tf_op | source)
XLA Modules:
  0.0 152.3 jit_solution(15890959232052903372)
XLA Ops:
  0.6 0.0 copy-start
  0.6 0.7 copy-done
  1.3 0.7 xor_bitcast_fusion
  2.1 0.8 bitcast_select_fusion
  2.8 0.7 copy.22
  3.5 0.7 copy.24.weight_cols_ref
  4.2 1.6 %copy.27 = bf16[32,8,2,128]{3,1,2,0:T(8,128)(2,1)} copy(bf16[32,8,2,128]{3,2,1,0:T(2,128)(2,1)} %bitcast.30) | data formatting | bytes 262144
  5.8 1.5 %maximum_bitcast_fusion.kv_ref = bf16[256,256]{1,0:T(8,128)(2,1)} fusion(bf16[256,1,128]{2,0,1:T(8,128)(2,1)} %param.15, bf16[256,1,128]{2,0,1:T(8,128)(2,1)} %param.14), kind=kLoop, calls=%fused_computation.2 | loop fusion | flops 262144 | bytes 262144 | tf_op jit(solution)/shard_map/reshape | solution.py:1010
  7.4 141.4 %shard_map.140 = (bf16[64,2048]{1,0:T(8,128)(2,1)}, bf16[128,2048]{1,0:T(8,128)(2,1)}) custom-call(bf16[4,128,2048]{2,1,0:T(8,128)(2,1)} %bitcast.34, f32[1,2048]{1,0:T(1,128)} %bitcast.38, s32[4,8,128]{2,1,0:T(8,128)} %get-tuple-element.4.places_ref, s32[128,8]{1,0:T(8,128)} %bitcast.32, f32[128,8]{1,0:T(8,128)} %copy.24.weight_cols_ref, ...), custom_call_target="tpu_custom_call" | custom-call | flops 257698037760 | bytes 16777216 | tf_op jit(solution)/shard_map/pallas_call | solution.py:931
  148.7 1.7 %copy.30 = bf16[64,2048]{1,0:T(8,128)(2,1)} copy(bf16[64,2048]{1,0:T(8,128)(2,1)} %get-tuple-element.8) | data formatting | bytes 524288
  150.4 1.9 %copy.31 = bf16[128,2048]{1,0:T(8,128)(2,1)} copy(bf16[128,2048]{1,0:T(8,128)(2,1)} %get-tuple-element.9) | data formatting | bytes 1048576
  (4 shorter events, 0.0 us)
Async XLA Ops:
  0.6 0.7 copy-start

commit v2 on v1

--- a/solution.py
+++ b/solution.py
@@ -413,11 +413,11 @@
     n,
     rows_ref,
     gain_ref,
-    places_ref,
-    place_cols_ref,
-    weight_cols_ref,
+    routes_ref,
+    weights_ref,
     q_ref,
-    kv_ref,
+    key_ref,
+    value_ref,
     lam_ref,
     head_gain_ref,
     gate_hbm,
@@ -433,17 +433,26 @@
     normed,
     packs,
     near_packs,
+    far_rows,
+    places_ref,
+    far_places,
+    scaled_ref,
+    cols_ref,
+    query_ref,
+    kv_ref,
     kv_all,
     slots,
     part,
     pair_in,
-    col_in,
     back,
     hidden_ref,
+    hidden_in,
+    down_peer,
     acc,
     run_max,
     run_total,
     run_acc,
+    head_rows,
     attn,
     heads_all,
     send_k,
@@ -464,6 +473,8 @@
     recv_r,
     send_h,
     recv_h,
+    send_x,
+    recv_x,
     local_sem,
 ):
     me = lax.axis_index("ep")
@@ -506,7 +517,6 @@
                 (gate_hbm, gate_ref),
                 (up_hbm, up_ref),
                 (down_hbm, down_ref),
-                (kv_ref, kv_all.at[me]),
                 (w_out_hbm, w_out_ref),
             )
         )
@@ -538,8 +548,7 @@
 
     slot_iota = lax.broadcasted_iota(jnp.int32, (slot_count, dev_rows), 0)
 
-    def take(b, first, last):
-        places = places_ref[b]
+    def take(places, first, last):
         return jnp.concatenate(
             [
                 jnp.where(places[d : d + 1, :] == slot_iota, 1.0, 0.0)
@@ -548,20 +557,35 @@
             axis=0,
         ).astype(jnp.bfloat16)
 
-    def select(b, taken, put):
-        @pl.loop(0, width // step)
-        def _(c):
-            cols = pl.ds(pl.multiple_of(c * step, step), step)
+    def select(source, taken, put, first=0, last=width // step):
+        for c in range(first, last):
+            cols = pl.ds(c * step, step)
             put(
                 cols,
                 jnp.dot(
-                    taken, normed[b, :, cols], preferred_element_type=jnp.float32
+                    taken, source[:, cols], preferred_element_type=jnp.float32
                 ).astype(packs.dtype),
             )
 
+    def copy_x(half):
+        cols = pl.ds(half * (width // 2), width // 2)
+        return remote(
+            normed.at[tp, :, cols],
+            far_rows.at[:, cols],
+            send_x.at[half],
+            recv_x.at[half],
+            partner(near),
+            tp,
+        )
+
+    def copy_m():
+        return remote(
+            places_ref.at[tp], far_places, send_x.at[2], recv_x.at[2], partner(near), tp
+        )
+
     def copy_a(d):
         return remote(
-            packs.at[d], slots.at[d, own_blk], send_a.at[d], recv_a.at[d], partner(d), tp
+            packs.at[d], slots.at[d, own_blk], send_a.at[d], recv_a.at[d], partner(d % near), tp
         )
 
     def copy_k(d):
@@ -588,22 +612,22 @@
         block = slots.at[d, far_blk]
         return remote(block, block, send_b.at[d], recv_b.at[d], me, pair_peer)
 
+    def copy_q(d):
+        return remote(
+            hidden_ref.at[d, other_row], hidden_in.at[d], send_q.at[d], recv_q.at[d], me, row_peer
+        )
+
     def copy_p(d):
         return remote(
-            part.at[d, pl.ds(other_col * 2, 2)],
-            pair_in.at[d],
-            send_p.at[d],
-            recv_p.at[d],
-            me,
-            pair_peer,
-        )
-
-    def copy_q(d):
-        return remote(part.at[d, far_blk], col_in.at[d], send_q.at[d], recv_q.at[d], me, row_peer)
+            part.at[d, other_col], pair_in.at[d], send_p.at[d], recv_p.at[d], me, pair_peer
+        )
+
+    def copy_w():
+        return remote(down_hbm, down_peer, send_x.at[3], recv_x.at[3], me, row_peer)
 
     def copy_r(d):
         return remote(
-            part.at[d, own_blk], back.at[d], send_r.at[d], recv_r.at[d], partner(d), tp
+            part.at[d, col], back.at[d], send_r.at[d], recv_r.at[d], partner(d), tp
         )
 
     positions = kv_ref.shape[0]
@@ -621,28 +645,51 @@
         )
 
     norm_block(tp)
-
-    def put_far(cols, val):
-        packs[near:n, :, cols] = val.reshape(n - near, slot_count, val.shape[1])
-
-    select(tp, take(tp, near, n), put_far)
     pl.semaphore_wait(barrier, n + 2)
-
-    @pl.loop(near, n)
-    def _(d):
-        copy_a(d).start()
-
-    loads[3].wait()
+    copy_x(0).start()
+    copy_x(1).start()
+    copy_w().start()
+
+    relative = jnp.bitwise_xor(routes_ref[...], me)
+    route_weights = weights_ref[...]
+    expert_iota = lax.broadcasted_iota(jnp.int32, (n, dev_rows), 0)
+    named = []
+    for b in range(4):
+        span = slice(b * dev_rows, (b + 1) * dev_rows)
+        hits = [relative[t : t + 1, span] == expert_iota for t in range(relative.shape[0])]
+        scaled_ref[b] = functools.reduce(
+            jnp.add,
+            [
+                jnp.where(hit, route_weights[t : t + 1, span], 0.0)
+                for t, hit in enumerate(hits)
+            ],
+        )
+        named.append(jnp.where(functools.reduce(jnp.logical_or, hits), 1.0, 0.0))
+    earlier = jnp.where(
+        lax.broadcasted_iota(jnp.int32, (dev_rows, dev_rows), 0)
+        < lax.broadcasted_iota(jnp.int32, (dev_rows, dev_rows), 1),
+        1.0,
+        0.0,
+    ).astype(jnp.bfloat16)
+    counts = jnp.dot(
+        jnp.concatenate(named, axis=0).astype(jnp.bfloat16),
+        earlier,
+        preferred_element_type=jnp.float32,
+    )
+    for b in range(4):
+        places_ref[b] = jnp.where(
+            named[b] > 0.5, counts[b * n : (b + 1) * n], -1.0
+        ).astype(jnp.int32)
+    copy_m().start()
+
+    kv_ref[:, : key_ref.shape[1]] = key_ref[...]
+    kv_ref[:, key_ref.shape[1] :] = value_ref[...]
     low = me < near
-
-    @pl.when(low)
-    def _():
-        copy_k(near).start()
 
     def put_near(cols, val):
         packs[0:near, :, cols] = val.reshape(near, slot_count, val.shape[1])
 
-    select(tp, take(tp, 0, near), put_near)
+    select(normed.at[tp], take(places_ref[tp], 0, near), put_near)
 
     @pl.loop(1, near)
     def _(d):
@@ -653,19 +700,12 @@
     def put_other(cols, val):
         near_packs[:, :, cols] = val.reshape(near, slot_count, val.shape[1])
 
-    select(row_peer, take(row_peer, 0, near), put_other)
-
-    @pl.loop(1, near)
-    def _(d):
-        copy_n(d).start()
-
-        @pl.when(partner(d) > me)
-        def _():
-            copy_k(d).start()
-
+    select(normed.at[row_peer], take(places_ref[row_peer], 0, near), put_other)
+
+    copy_n(1).start()
     fills = [
-        pltpu.make_async_copy(packs.at[0], slots.at[0, own_blk], local_sem.at[5]),
-        pltpu.make_async_copy(near_packs.at[0], slots.at[0, far_blk], local_sem.at[6]),
+        pltpu.make_async_copy(packs.at[0], slots.at[0, own_blk], local_sem.at[4]),
+        pltpu.make_async_copy(near_packs.at[0], slots.at[0, far_blk], local_sem.at[5]),
     ]
     for fill in fills:
         fill.start()
@@ -677,39 +717,72 @@
         def put_mine(cols, val, peer_row=peer_row):
             slots[0, other_col * 2 + peer_row, :, cols] = val
 
-        select(block, take(block, 0, 1), put_mine)
+        select(normed.at[block], take(places_ref[block], 0, 1), put_mine)
     for fill in fills:
         fill.wait()
     for load in loads[:3]:
         load.wait()
 
-    def merge(index, other):
-        rows = part.at[index]
-
-        @pl.loop(0, width // step)
-        def _(c):
-            cols = pl.ds(pl.multiple_of(c * step, step), step)
-            rows[:, cols] = (
-                rows[:, cols].astype(jnp.float32) + other[:, cols].astype(jnp.float32)
+    def merge(j):
+        for c in range(width // step):
+            cols = pl.ds(c * step, step)
+            part[j, col, :, cols] = (
+                part[j, col, :, cols].astype(jnp.float32)
+                + pair_in[j, :, cols].astype(jnp.float32)
             ).astype(part.dtype)
 
-    def compute(j):
-        rows = slots[j].reshape(4 * slot_count, width)
+    def hidden_half(j, side):
+        rows = slots[j, pl.ds(side * 2, 2)].reshape(2 * slot_count, width)
         gate = jnp.dot(rows, gate_ref[...], preferred_element_type=jnp.float32)
         up = jnp.dot(rows, up_ref[...], preferred_element_type=jnp.float32)
-        hidden_ref[...] = (gate / (1.0 + jnp.exp(-gate)) * up).astype(hidden_ref.dtype)
-
-        @pl.loop(0, width // step)
-        def _(c):
-            cols = pl.ds(pl.multiple_of(c * step, step), step)
+        hidden = (gate / (1.0 + jnp.exp(-gate)) * up).astype(hidden_ref.dtype)
+        hidden_ref[j, 0, side] = hidden[:slot_count]
+        hidden_ref[j, 1, side] = hidden[slot_count:]
+
+    def down(j):
+        units = down_ref.shape[0]
+        mine = hidden_ref[j, row].reshape(2 * slot_count, units)
+        other = hidden_in[j].reshape(2 * slot_count, units)
+        for c in range(width // step):
+            cols = pl.ds(c * step, step)
             val = jnp.dot(
-                hidden_ref[...], down_ref[:, cols], preferred_element_type=jnp.float32
-            ).astype(part.dtype)
-            part[j, :, :, cols] = val.reshape(4, slot_count, step)
+                mine, down_ref[:, cols], preferred_element_type=jnp.float32
+            ) + jnp.dot(other, down_peer[:, cols], preferred_element_type=jnp.float32)
+            part[j, :, :, cols] = val.astype(part.dtype).reshape(2, slot_count, step)
+
+    def spread_far():
+        copy_m().wait_recv()
+        taken = take(far_places[...], near, n)
+
+        def put_far(cols, val):
+            packs[near:n, :, cols] = val.reshape(n - near, slot_count, val.shape[1])
+            slots[near, own_blk, :, cols] = val[:slot_count]
+
+        for half in range(2):
+            copy_x(half).wait_recv()
+            chunks = width // step // 2
+            select(far_rows, taken, put_far, half * chunks, (half + 1) * chunks)
+
+        @pl.loop(near + 1, n)
+        def _(d):
+            copy_a(d).start()
+
+        @pl.loop(2, near)
+        def _(d):
+            copy_n(d).start()
+
+        @pl.when(low)
+        def _():
+            copy_k(near).start()
+
+        @pl.loop(1, near)
+        def _(d):
+            @pl.when(partner(d) > me)
+            def _():
+                copy_k(d).start()
 
     def order(i):
-        far_step = near + i - 1
-        return jnp.where(i <= 0, 0, jnp.where(i <= near, far_step, i - near))
+        return jnp.where(i < 2, i, jnp.where(i < near + 2, near - 2 + i, i - near))
 
     def inside(j, low_bound):
         return jnp.logical_and(j >= low_bound, j < n)
@@ -720,50 +793,67 @@
         d_mid = order(i - 1)
         d_out = order(i - 2)
 
+        @pl.when(i == 2)
+        def _():
+            spread_far()
+
         @pl.when(inside(i, 1))
         def _():
-            copy_a(d_in).wait_recv()
+            @pl.when(d_in != near)
+            def _():
+                copy_a(d_in).wait_recv()
+
             copy_c(d_in).start()
 
             @pl.when(d_in >= near)
             def _():
                 copy_y(d_in).start()
 
-        @pl.when(inside(i - 1, 1))
-        def _():
-            copy_y(d_mid).wait_recv()
-            copy_b(d_mid).start()
-            copy_c(d_mid).wait_recv()
-            copy_b(d_mid).wait_recv()
-
-        @pl.when(inside(i - 1, 0))
-        def _():
-            compute(d_mid)
-            copy_p(d_mid).start()
-
-        @pl.when(inside(i - 2, 0))
-        def _():
-            copy_q(d_out).wait_recv()
-            merge((d_out, own_blk), col_in.at[d_out])
-
-        @pl.when(inside(i - 2, 1))
-        def _():
-            copy_r(d_out).start()
-
-        @pl.when(inside(i - 1, 0))
-        def _():
-            copy_p(d_mid).wait_recv()
-            for y in range(2):
-                merge((d_mid, col * 2 + y), pair_in.at[d_mid, y])
-            copy_q(d_mid).start()
-
-        @pl.when(jnp.logical_and(i == near + 1, jnp.logical_not(low)))
+        @pl.when(jnp.logical_and(i == n - 1, jnp.logical_not(low)))
         def _():
             copy_k(near).wait_recv()
 
             @pl.loop(near + 1, n)
             def _(d):
                 copy_f(d).start()
+
+        @pl.when(i == 2)
+        def _():
+            copy_w().wait_recv()
+
+        @pl.when(inside(i - 2, 0))
+        def _():
+            copy_q(d_out).wait_recv()
+            down(d_out)
+            copy_p(d_out).start()
+
+        @pl.when(inside(i - 2, 0))
+        def _():
+            copy_p(d_out).wait_recv()
+            merge(d_out)
+
+        @pl.when(inside(i - 2, 1))
+        def _():
+            copy_r(d_out).start()
+
+        @pl.when(inside(i - 1, 1))
+        def _():
+            copy_y(d_mid).wait_recv()
+            copy_b(d_mid).start()
+
+        @pl.when(inside(i - 1, 0))
+        def _():
+            hidden_half(d_mid, col)
+
+        @pl.when(inside(i - 1, 1))
+        def _():
+            copy_c(d_mid).wait_recv()
+            copy_b(d_mid).wait_recv()
+
+        @pl.when(inside(i - 1, 0))
+        def _():
+            hidden_half(d_mid, other_col)
+            copy_q(d_mid).start()
 
     @pl.loop(1, near)
     def _(d):
@@ -778,49 +868,55 @@
             copy_f(d).wait_recv()
 
     head_dim2 = kv_ref.shape[1] // 2
-    q_heads = q_ref.shape[1] // head_dim2
+    q_heads = q_ref.shape[0] // positions
     inv_scale = (head_dim2 // 2) ** (-0.5)
+    head_rows[...] = q_ref[...].astype(jnp.float32)
+    map_of = lax.broadcasted_iota(jnp.int32, (positions, head_dim2), 1) // (head_dim2 // 2)
+    for h in range(q_heads):
+        query = head_rows[pl.ds(h, positions, stride=q_heads), :] * inv_scale
+        for m in range(2):
+            query_ref[2 * h + m] = jnp.where(map_of == m, query, 0.0).astype(query_ref.dtype)
     run_max[...] = jnp.full(run_max.shape, MASKED, jnp.float32)
     run_total[...] = jnp.zeros(run_total.shape, jnp.float32)
     run_acc[...] = jnp.zeros(run_acc.shape, jnp.float32)
-    map_of = lax.broadcasted_iota(jnp.int32, (positions, head_dim2), 1) // (head_dim2 // 2)
-
-    @pl.loop(0, me + 1)
+
+    def visit(block, masked):
+        keys = block[:, :head_dim2]
+        vals = block[:, head_dim2:]
+        for at in range(2 * q_heads):
+            scores = lax.dot_general(
+                keys, query_ref[at], (((1,), (1,)), ((), ())), preferred_element_type=jnp.float32
+            )
+            if masked:
+                allowed = lax.broadcasted_iota(
+                    jnp.int32, (positions, positions), 0
+                ) <= lax.broadcasted_iota(jnp.int32, (positions, positions), 1)
+                scores = jnp.where(allowed, scores, MASKED)
+            old_max = run_max[at : at + 1]
+            new_max = jnp.maximum(old_max, jnp.max(scores, axis=0, keepdims=True))
+            shrink = jnp.exp(old_max - new_max)
+            weights = jnp.exp(scores - new_max)
+            run_max[at : at + 1] = new_max
+            run_total[at : at + 1] = run_total[at : at + 1] * shrink + jnp.sum(
+                weights, axis=0, keepdims=True
+            )
+            run_acc[at] = run_acc[at] * shrink + lax.dot_general(
+                vals,
+                weights.astype(jnp.bfloat16),
+                (((0,), (0,)), ((), ())),
+                preferred_element_type=jnp.float32,
+            )
+
+    visit(kv_ref, True)
+
+    @pl.loop(0, me)
     def _(kb):
-        keys = kv_all[kb, :, :head_dim2]
-        vals = kv_all[kb, :, head_dim2:]
-        gap = (me - kb) * positions
-        allowed = (
-            lax.broadcasted_iota(jnp.int32, (positions, positions), 1)
-            <= lax.broadcasted_iota(jnp.int32, (positions, positions), 0) + gap
-        )
-        for h in range(q_heads):
-            for m in range(2):
-                at = h * 2 + m
-                query = q_ref[:, h * head_dim2 : (h + 1) * head_dim2]
-                query = jnp.where(map_of == m, query, jnp.zeros_like(query))
-                scores = (
-                    lax.dot_general(
-                        query, keys, (((1,), (1,)), ((), ())), preferred_element_type=jnp.float32
-                    )
-                    * inv_scale
-                )
-                scores = jnp.where(allowed, scores, MASKED)
-                old_max = run_max[at]
-                new_max = jnp.maximum(old_max, jnp.max(scores, axis=1, keepdims=True))
-                shrink = jnp.exp(old_max - new_max)
-                weights = jnp.exp(scores - new_max)
-                run_max[at] = new_max
-                run_total[at] = run_total[at] * shrink + jnp.sum(weights, axis=1, keepdims=True)
-                run_acc[at] = run_acc[at] * shrink + jnp.dot(
-                    weights.astype(jnp.bfloat16), vals, preferred_element_type=jnp.float32
-                )
+        visit(kv_all.at[kb], False)
 
     for h in range(q_heads):
-        head_out = (
-            run_acc[2 * h] / run_total[2 * h]
-            - lam_ref[h] * run_acc[2 * h + 1] / run_total[2 * h + 1]
-        )
+        first = run_acc[2 * h] / run_total[2 * h : 2 * h + 1]
+        second = run_acc[2 * h + 1] / run_total[2 * h + 1 : 2 * h + 2]
+        head_out = jnp.transpose(first - lam_ref[h] * second)
         attn[:, h * head_dim2 : (h + 1) * head_dim2] = rms_scaled(
             head_out, head_gain_ref[...]
         ).astype(attn.dtype)
@@ -829,39 +925,45 @@
         copy_h(t).start()
     heads_all[tp] = attn[pl.ds(pl.multiple_of(tp * piece_rows, piece_rows), piece_rows), :]
 
-    def collect(d, rows):
-        lanes = lax.broadcasted_iota(jnp.int32, place_cols_ref.shape, 1)
-        place = jnp.sum(jnp.where(lanes == d, place_cols_ref[...], 0), axis=1, keepdims=True)
-        weight = jnp.sum(jnp.where(lanes == d, weight_cols_ref[...], 0.0), axis=1, keepdims=True)
-        slot = lax.broadcasted_iota(jnp.int32, (dev_rows, slot_count), 1)
-        mix = jnp.where(slot == place, weight, 0.0)
+    spare = jnp.zeros((dev_rows - 2 * n, dev_rows), jnp.float32)
+    cols_ref[...] = jnp.transpose(
+        jnp.concatenate([places_ref[tp].astype(jnp.float32), scaled_ref[tp], spare], axis=0)
+    )
+
+    def collect(first, last, rows):
+        lanes = lax.broadcasted_iota(jnp.int32, cols_ref.shape, 1)
+        slot = lax.broadcasted_iota(jnp.int32, (dev_rows, slot_count), 1).astype(jnp.float32)
+        mixes = []
+        for d in range(first, last):
+            place = jnp.sum(jnp.where(lanes == d, cols_ref[...], 0.0), axis=1, keepdims=True)
+            weight = jnp.sum(jnp.where(lanes == d + n, cols_ref[...], 0.0), axis=1, keepdims=True)
+            mixes.append(jnp.where(slot == place, weight, 0.0))
+        mix = jnp.concatenate(mixes, axis=1)
         high = mix.astype(jnp.bfloat16)
         low_part = (mix - high.astype(jnp.float32)).astype(jnp.bfloat16)
-
-        @pl.loop(0, width // step)
-        def _(c):
-            cols = pl.ds(pl.multiple_of(c * step, step), step)
-            piece = rows[:, cols]
+        for c in range(width // step):
+            cols = pl.ds(c * step, step)
+            piece = rows[..., cols].reshape((last - first) * slot_count, step)
             acc[:, cols] += jnp.dot(high, piece, preferred_element_type=jnp.float32) + jnp.dot(
                 low_part, piece, preferred_element_type=jnp.float32
             )
 
     acc[...] = jnp.zeros(acc.shape, jnp.float32)
-    collect(0, part.at[0, own_blk])
+    collect(0, 1, part.at[0, col])
 
     @pl.loop(1, near)
     def _(d):
         copy_r(d).wait_recv()
-        collect(d, back.at[d])
-
-    loads[4].wait()
+
+    collect(1, near, back.at[1:near])
+
+    loads[3].wait()
     for t in range(1, 4):
         copy_h(t).wait_recv()
     mixed = heads_all.shape[2]
 
-    @pl.loop(0, width // step)
-    def _(c):
-        cols = pl.ds(pl.multiple_of(c * step, step), step)
+    for c in range(width // step):
+        cols = pl.ds(c * step, step)
         total = jnp.zeros((piece_rows, step), jnp.float32)
         for t in range(4):
             total = total + jnp.dot(
@@ -874,7 +976,8 @@
     @pl.loop(near, n)
     def _(d):
         copy_r(d).wait_recv()
-        collect(d, back.at[d])
+
+    collect(near, n, back.at[near:n])
 
     res_ref[...] = acc[...].astype(res_ref.dtype)
 
@@ -900,9 +1003,17 @@
     def _(d):
         copy_y(d).wait_send()
 
+    for half in range(2):
+        copy_x(half).wait_send()
+    copy_m().wait_send()
+    copy_w().wait_send()
+
     @pl.loop(1, n)
     def _(d):
-        copy_a(d).wait_send()
+        @pl.when(d != near)
+        def _():
+            copy_a(d).wait_send()
+
         copy_c(d).wait_send()
         copy_b(d).wait_send()
         copy_r(d).wait_send()
@@ -916,13 +1027,14 @@
         copy_h(t).wait_send()
 
 
-def run_layer(n, capacity, rows, gain, places, place_cols, weight_cols, q, kv, lam, head_gain, mats):
+def run_layer(n, capacity, rows, gain, routes, weights, q, keys, values, lam, head_gain, mats):
     tp_count, dev_rows, width = rows.shape
     gate_w, up_w, down_w, w_out = mats
     hidden_units = gate_w.shape[1]
-    positions, mixed = q.shape
-    head_dim2 = kv.shape[1] // 2
-    maps = 2 * mixed // head_dim2
+    positions, head_dim2 = keys.shape
+    q_heads = q.shape[0] // positions
+    mixed = q_heads * head_dim2
+    maps = 2 * q_heads
     dtype = rows.dtype
     near = n // 2
     vmem = pl.BlockSpec(memory_space=pltpu.VMEM)
@@ -944,30 +1056,39 @@
             pltpu.VMEM((tp_count, dev_rows, width), dtype),
             pltpu.VMEM((n, capacity, width), dtype),
             pltpu.VMEM((near, capacity, width), dtype),
-            pltpu.VMEM((n,) + kv.shape, dtype),
-            pltpu.VMEM((n, 4, capacity, width), dtype),
+            pltpu.VMEM((dev_rows, width), dtype),
+            pltpu.VMEM((tp_count, n, dev_rows), jnp.int32),
+            pltpu.VMEM((n, dev_rows), jnp.int32),
+            pltpu.VMEM((tp_count, n, dev_rows), jnp.float32),
+            pltpu.VMEM((dev_rows, dev_rows), jnp.float32),
+            pltpu.VMEM((maps, positions, head_dim2), dtype),
+            pltpu.VMEM((positions, 2 * head_dim2), dtype),
+            pltpu.VMEM((n, positions, 2 * head_dim2), dtype),
             pltpu.VMEM((n, 4, capacity, width), dtype),
             pltpu.VMEM((n, 2, capacity, width), dtype),
             pltpu.VMEM((n, capacity, width), dtype),
             pltpu.VMEM((n, capacity, width), dtype),
-            pltpu.VMEM((4 * capacity, hidden_units), dtype),
+            pltpu.VMEM((n, 2, 2, capacity, hidden_units), dtype),
+            pltpu.VMEM((n, 2, capacity, hidden_units), dtype),
+            pltpu.VMEM(down_w.shape, dtype),
             pltpu.VMEM((dev_rows, width), jnp.float32),
-            pltpu.VMEM((maps, positions, 1), jnp.float32),
-            pltpu.VMEM((maps, positions, 1), jnp.float32),
-            pltpu.VMEM((maps, positions, head_dim2), jnp.float32),
+            pltpu.VMEM((maps, positions), jnp.float32),
+            pltpu.VMEM((maps, positions), jnp.float32),
+            pltpu.VMEM((maps, head_dim2, positions), jnp.float32),
+            pltpu.VMEM(q.shape, jnp.float32),
             pltpu.VMEM((positions, mixed), dtype),
             pltpu.VMEM((tp_count, positions // tp_count, mixed), dtype),
         ]
         + [pltpu.SemaphoreType.DMA((n,))] * 16
-        + [pltpu.SemaphoreType.DMA((4,))] * 2
-        + [pltpu.SemaphoreType.DMA((7,))],
+        + [pltpu.SemaphoreType.DMA((4,))] * 4
+        + [pltpu.SemaphoreType.DMA((6,))],
         compiler_params=pltpu.CompilerParams(
             collective_id=1, has_side_effects=True, vmem_limit_bytes=60 * 1024 * 1024
         ),
         cost_estimate=pl.CostEstimate(
             flops=40 * flops, bytes_accessed=16 * 1024 * 1024, transcendentals=0
         ),
-    )(rows, gain, places, place_cols, weight_cols, q, kv, lam, head_gain, *mats)
+    )(rows, gain, routes, weights, q, keys, values, lam, head_gain, *mats)
 
 
 def one_kernel(
@@ -987,39 +1108,22 @@
 ):
     experts = lax.axis_size("ep")
     tp_count = lax.axis_size("tp")
-    me = lax.axis_index("ep")
-    tp_id = lax.axis_index("tp")
-    positions = queries.shape[0]
+    positions, q_heads, head_dim2 = queries.shape
     width = moe_rows.shape[1]
     dev_rows = moe_rows.shape[0] // tp_count
-    top_count = routes.shape[1]
-    capacity = 2 * dev_rows * top_count // experts
-    relative = jnp.bitwise_xor(routes, me).reshape(tp_count, dev_rows, top_count)
-    hits = relative[..., None] == lax.iota(jnp.int32, experts)
-    named = jnp.any(hits, axis=2)
-    before = (
-        lax.iota(jnp.int32, dev_rows)[:, None] > lax.iota(jnp.int32, dev_rows)[None, :]
-    ).astype(jnp.bfloat16)
-    places = jnp.einsum(
-        "ij,bjd->bid", before, named.astype(jnp.bfloat16), preferred_element_type=jnp.float32
-    ).astype(jnp.int32)
-    places = jnp.where(named, places, -1)
-    own = lambda arr: lax.dynamic_index_in_dim(arr, tp_id, 0, keepdims=False)
-    own_weights = own(route_weights.reshape(tp_count, dev_rows, top_count))
-    weight_cols = jnp.sum(jnp.where(own(hits), own_weights[..., None], 0.0), axis=1)
-    kv = jnp.concatenate([keys, values], axis=2).reshape(positions, -1)
+    capacity = 2 * dev_rows * routes.shape[1] // experts
     return run_layer(
         experts,
         capacity,
         moe_rows.reshape(tp_count, dev_rows, width),
         moe_gain.reshape(1, width),
-        jnp.transpose(places, (0, 2, 1)),
-        own(places),
-        weight_cols,
-        queries.reshape(positions, -1),
-        kv,
+        routes.T,
+        route_weights.T,
+        queries.reshape(positions * q_heads, head_dim2),
+        keys.reshape(positions, head_dim2),
+        values.reshape(positions, head_dim2),
         attn_lambda,
-        head_gain.reshape(1, -1),
+        head_gain.reshape(1, head_dim2),
         (w_gate[0], w_up[0], w_down[0], w_out),
     )
 

time: 154 us -> 111 us (0.72)
  Pallas kernels: 141 us -> 106 us
  local copies, waits for them, and re-layouts: 7.24 us -> 3.55 us
  other arithmetic: 2.26 us -> 0 us
    pallas_call x1, Pallas kernels: 141 us -> 106 us  [run_layer(): pl.pallas_call(functools.partial(layer_kernel, n), out_shape=(jax.ShapeDt...]
    unnamed x5 -> x2, local copies, waits for them, and re-layouts: 5.81 us -> 3.55 us
    reshape x1 -> x0, other arithmetic: 1.54 us -> none  [one_kernel(): kv = jnp.concatenate([keys, values], axis=2).reshape(positions, -1)]
where the time goes in v2:
time: 111 us
  Pallas kernels  106 us (95%)
  local copies, waits for them, and re-layouts  3.55 us (3%)
    pallas_call x1, Pallas kernels, run_layer(): pl.pallas_call(functools.partial(layer_kernel, n), out_shape=(jax.ShapeDt...  106 us
    unnamed x2, local copies, waits for them, and re-layouts  3.55 us

profile of v2, /device:TPU:27, one launch (start us, length us, event | category | flops | bytes accessed | tf_op | source)
XLA Modules:
  0.0 110.6 jit_solution(17917449671540902820)
XLA Ops:
  0.6 106.5 %shard_map.140 = (bf16[64,2048]{1,0:T(8,128)(2,1)}, bf16[128,2048]{1,0:T(8,128)(2,1)}) custom-call(bf16[4,128,2048]{2,1,0:T(8,128)(2,1)} %bitcast.11, f32[1,2048]{1,0:T(1,128)} %bitcast.18, s32[2,512]{1,0:T(2,128)} %bitcast.19, f32[2,512]{1,0:T(2,128)} %bitcast.20, bf16[512,128]{1,0:T(8,128)(2,1)} %bitcast.15, bf16[256,128]{1,0:T(8,128)(2,1)} %bitcast.16, ...), custom_call_target="tpu_custom_call" | custom-call | flops 257698037760 | bytes 16777216 | tf_op jit(solution)/shard_map/pallas_call | solution.py:1043
  107.1 1.7 %copy.17 = bf16[64,2048]{1,0:T(8,128)(2,1)} copy(bf16[64,2048]{1,0:T(8,128)(2,1)} %get-tuple-element.4) | data formatting | bytes 524288
  108.8 1.9 %copy.18 = bf16[128,2048]{1,0:T(8,128)(2,1)} copy(bf16[128,2048]{1,0:T(8,128)(2,1)} %get-tuple-element.5) | data formatting | bytes 1048576

commit v3 on v2

--- a/solution.py
+++ b/solution.py
@@ -475,6 +475,8 @@
     recv_h,
     send_x,
     recv_x,
+    send_s,
+    recv_s,
     local_sem,
 ):
     me = lax.axis_index("ep")
@@ -585,8 +587,25 @@
 
     def copy_a(d):
         return remote(
-            packs.at[d], slots.at[d, own_blk], send_a.at[d], recv_a.at[d], partner(d % near), tp
-        )
+            packs.at[d], slots.at[d, own_blk], send_a.at[d], recv_a.at[d], partner(d), tp
+        )
+
+    def half_cols(half):
+        return pl.ds(half * (width // 2), width // 2)
+
+    def copy_ah(d, half):
+        return remote(
+            packs.at[d, :, half_cols(half)],
+            slots.at[d, own_blk, :, half_cols(half)],
+            send_s.at[d, half],
+            recv_s.at[d, half],
+            partner(d % near),
+            tp,
+        )
+
+    def copy_yh(half):
+        block = slots.at[near, own_blk, :, half_cols(half)]
+        return remote(block, block, send_s.at[near, half], recv_s.at[near, half], me, row_peer)
 
     def copy_k(d):
         return remote(kv_ref, kv_all.at[me], send_k.at[d], recv_k.at[d], partner(d), tp)
@@ -594,6 +613,13 @@
     def copy_f(d):
         block = kv_all.at[partner(near)]
         return remote(block, block, send_k.at[d], recv_k.at[d], partner(d - near), tp)
+
+    def copy_g(d):
+        block = kv_all.at[partner(d - 1)]
+        return remote(block, block, send_k.at[d], recv_k.at[d], partner(1), tp)
+
+    direct = [d for d in range(1, near) if d == 1 or d % 2 == 0]
+    relayed = [d for d in range(1, near) if d > 1 and d % 2]
 
     def copy_n(d):
         return remote(
@@ -698,9 +724,9 @@
     norm_block(row_peer)
 
     def put_other(cols, val):
-        near_packs[:, :, cols] = val.reshape(near, slot_count, val.shape[1])
-
-    select(normed.at[row_peer], take(places_ref[row_peer], 0, near), put_other)
+        near_packs[:, :, cols] = val.reshape(3, slot_count, val.shape[1])
+
+    select(normed.at[row_peer], take(places_ref[row_peer], 0, 3), put_other)
 
     copy_n(1).start()
     fills = [
@@ -762,23 +788,23 @@
             copy_x(half).wait_recv()
             chunks = width // step // 2
             select(far_rows, taken, put_far, half * chunks, (half + 1) * chunks)
-
-        @pl.loop(near + 1, n)
-        def _(d):
-            copy_a(d).start()
-
-        @pl.loop(2, near)
-        def _(d):
-            copy_n(d).start()
+            if half == 0:
+                copy_yh(0).start()
+
+            @pl.loop(near + 1, n)
+            def _(d):
+                copy_ah(d, half).start()
+
+        copy_n(2).start()
 
         @pl.when(low)
         def _():
             copy_k(near).start()
 
-        @pl.loop(1, near)
-        def _(d):
+        for d in direct:
+
             @pl.when(partner(d) > me)
-            def _():
+            def _(d=d):
                 copy_k(d).start()
 
     def order(i):
@@ -799,23 +825,45 @@
 
         @pl.when(inside(i, 1))
         def _():
-            @pl.when(d_in != near)
+            @pl.when(d_in < near)
             def _():
                 copy_a(d_in).wait_recv()
 
+            @pl.when(d_in > near)
+            def _():
+                for half in range(2):
+                    copy_ah(d_in, half).wait_recv()
+
             copy_c(d_in).start()
 
-            @pl.when(d_in >= near)
+            @pl.when(d_in == near)
+            def _():
+                copy_yh(1).start()
+
+            @pl.when(jnp.logical_and(d_in >= 3, d_in != near))
             def _():
                 copy_y(d_in).start()
 
-        @pl.when(jnp.logical_and(i == n - 1, jnp.logical_not(low)))
+        @pl.when(jnp.logical_and(i == n - 2, jnp.logical_not(low)))
         def _():
             copy_k(near).wait_recv()
-
-            @pl.loop(near + 1, n)
-            def _(d):
-                copy_f(d).start()
+            for d in direct:
+                copy_f(near + d).start()
+
+        @pl.when(i == n - 1)
+        def _():
+            for d in relayed:
+
+                @pl.when(partner(d - 1) < me)
+                def _(d=d):
+                    copy_k(d - 1).wait_recv()
+                    copy_g(d).start()
+
+        @pl.when(jnp.logical_and(i == n, jnp.logical_not(low)))
+        def _():
+            for d in relayed:
+                copy_f(near + d - 1).wait_recv()
+                copy_g(near + d).start()
 
         @pl.when(i == 2)
         def _():
@@ -827,6 +875,23 @@
             down(d_out)
             copy_p(d_out).start()
 
+        @pl.when(inside(i - 1, 1))
+        def _():
+            @pl.when(d_mid != near)
+            def _():
+                copy_y(d_mid).wait_recv()
+
+            @pl.when(d_mid == near)
+            def _():
+                for half in range(2):
+                    copy_yh(half).wait_recv()
+
+            copy_b(d_mid).start()
+
+        @pl.when(inside(i - 1, 0))
+        def _():
+            hidden_half(d_mid, col)
+
         @pl.when(inside(i - 2, 0))
         def _():
             copy_p(d_out).wait_recv()
@@ -838,15 +903,6 @@
 
         @pl.when(inside(i - 1, 1))
         def _():
-            copy_y(d_mid).wait_recv()
-            copy_b(d_mid).start()
-
-        @pl.when(inside(i - 1, 0))
-        def _():
-            hidden_half(d_mid, col)
-
-        @pl.when(inside(i - 1, 1))
-        def _():
             copy_c(d_mid).wait_recv()
             copy_b(d_mid).wait_recv()
 
@@ -855,17 +911,19 @@
             hidden_half(d_mid, other_col)
             copy_q(d_mid).start()
 
-    @pl.loop(1, near)
-    def _(d):
-        @pl.when(partner(d) < me)
-        def _():
-            copy_k(d).wait_recv()
+    waited = [d - 1 for d in relayed]
+    for d in range(1, near):
+        if d not in waited:
+
+            @pl.when(partner(d) < me)
+            def _(d=d):
+                copy_k(d).wait_recv()
 
     @pl.when(jnp.logical_not(low))
     def _():
-        @pl.loop(near + 1, n)
-        def _(d):
-            copy_f(d).wait_recv()
+        for d in range(1, near):
+            if d not in waited:
+                copy_f(near + d).wait_recv()
 
     head_dim2 = kv_ref.shape[1] // 2
     q_heads = q_ref.shape[0] // positions
@@ -985,23 +1043,35 @@
     def _():
         copy_k(near).wait_send()
 
-    @pl.loop(1, near)
-    def _(d):
-        copy_n(d).wait_send()
+    for d in direct:
 
         @pl.when(partner(d) > me)
-        def _():
+        def _(d=d):
             copy_k(d).wait_send()
+
+    for d in relayed:
+
+        @pl.when(partner(d - 1) < me)
+        def _(d=d):
+            copy_g(d).wait_send()
 
     @pl.when(jnp.logical_not(low))
     def _():
-        @pl.loop(near + 1, n)
-        def _(d):
-            copy_f(d).wait_send()
-
-    @pl.loop(near, n)
-    def _(d):
-        copy_y(d).wait_send()
+        for d in direct:
+            copy_f(near + d).wait_send()
+        for d in relayed:
+            copy_g(near + d).wait_send()
+
+    for d in (1, 2):
+        copy_n(d).wait_send()
+    for half in range(2):
+        copy_yh(half).wait_send()
+
+    @pl.loop(3, n)
+    def _(d):
+        @pl.when(d != near)
+        def _():
+            copy_y(d).wait_send()
 
     for half in range(2):
         copy_x(half).wait_send()
@@ -1010,9 +1080,14 @@
 
     @pl.loop(1, n)
     def _(d):
-        @pl.when(d != near)
+        @pl.when(d < near)
         def _():
             copy_a(d).wait_send()
+
+        @pl.when(d > near)
+        def _():
+            for half in range(2):
+                copy_ah(d, half).wait_send()
 
         copy_c(d).wait_send()
         copy_b(d).wait_send()
@@ -1025,6 +1100,11 @@
 
     for t in range(1, 4):
         copy_h(t).wait_send()
+
+
+def settle_kernel(mixer_in, moe_in, mixer_ref, moe_ref):
+    mixer_ref[...] = mixer_in[...]
+    moe_ref[...] = moe_in[...]
 
 
 def run_layer(n, capacity, rows, gain, routes, weights, q, keys, values, lam, head_gain, mats):
@@ -1040,7 +1120,7 @@
     vmem = pl.BlockSpec(memory_space=pltpu.VMEM)
     hbm = pl.BlockSpec(memory_space=pl.ANY)
     flops = 2 * n * 4 * capacity * width * hidden_units * 3
-    return pl.pallas_call(
+    outs = pl.pallas_call(
         functools.partial(layer_kernel, n),
         out_shape=(
             jax.ShapeDtypeStruct((positions // tp_count, width), dtype),
@@ -1055,7 +1135,7 @@
             pltpu.VMEM(w_out.shape, dtype),
             pltpu.VMEM((tp_count, dev_rows, width), dtype),
             pltpu.VMEM((n, capacity, width), dtype),
-            pltpu.VMEM((near, capacity, width), dtype),
+            pltpu.VMEM((3, capacity, width), dtype),
             pltpu.VMEM((dev_rows, width), dtype),
             pltpu.VMEM((tp_count, n, dev_rows), jnp.int32),
             pltpu.VMEM((n, dev_rows), jnp.int32),
@@ -1081,6 +1161,7 @@
         ]
         + [pltpu.SemaphoreType.DMA((n,))] * 16
         + [pltpu.SemaphoreType.DMA((4,))] * 4
+        + [pltpu.SemaphoreType.DMA((n, 2))] * 2
         + [pltpu.SemaphoreType.DMA((6,))],
         compiler_params=pltpu.CompilerParams(
             collective_id=1, has_side_effects=True, vmem_limit_bytes=60 * 1024 * 1024
@@ -1089,6 +1170,12 @@
             flops=40 * flops, bytes_accessed=16 * 1024 * 1024, transcendentals=0
         ),
     )(rows, gain, routes, weights, q, keys, values, lam, head_gain, *mats)
+    return pl.pallas_call(
+        settle_kernel,
+        out_shape=tuple(jax.ShapeDtypeStruct(o.shape, o.dtype) for o in outs),
+        in_specs=[vmem] * 2,
+        out_specs=(vmem, vmem),
+    )(*outs)
 
 
 def one_kernel(

time: 111 us -> 105 us (0.946); the launches traced: 111 us -> 103 us
  local copies, waits for them, and re-layouts: 3.55 us -> 0 us
  Pallas kernels: 106 us -> 103 us
    pallas_call x1, Pallas kernels: 106 us -> 101 us  [run_layer(): pl.pallas_call(functools.partial(layer_kernel, n), out_shape=(jax.ShapeDt...]
    unnamed x2 -> x0, local copies, waits for them, and re-layouts: 3.55 us -> none
    pallas_call x0 -> x1, Pallas kernels: none -> 2.02 us  [run_layer(): pl.pallas_call(settle_kernel, out_shape=tuple((jax.ShapeDtypeStruct(o.sha...]
where the time goes in v3:
time: 105 us; the launch traced here: 103 us
  Pallas kernels  103 us (98%)
    pallas_call x1, Pallas kernels, run_layer(): pl.pallas_call(functools.partial(layer_kernel, n), out_shape=(jax.ShapeDt...  101 us

profile of v3, /device:TPU:27, one launch (start us, length us, event | category | flops | bytes accessed | tf_op | source)
XLA Modules:
  0.0 103.2 jit_solution(16949958598792486150)
XLA Ops:
  0.6 100.5 %shard_map.140 = (bf16[64,2048]{1,0:T(8,128)(2,1)}, bf16[128,2048]{1,0:T(8,128)(2,1)}) custom-call(bf16[4,128,2048]{2,1,0:T(8,128)(2,1)} %bitcast.11, f32[1,2048]{1,0:T(1,128)} %bitcast.18, s32[2,512]{1,0:T(2,128)} %bitcast.19, f32[2,512]{1,0:T(2,128)} %bitcast.20, bf16[512,128]{1,0:T(8,128)(2,1)} %bitcast.15, bf16[256,128]{1,0:T(8,128)(2,1)} %bitcast.16, ...), custom_call_target="tpu_custom_call" | custom-call | flops 257698037760 | bytes 16777216 | tf_op jit(solution)/shard_map/pallas_call | solution.py:1123
  101.2 2.0 %shard_map.141 = (bf16[64,2048]{1,0:T(8,128)(2,1)}, bf16[128,2048]{1,0:T(8,128)(2,1)}) custom-call(bf16[64,2048]{1,0:T(8,128)(2,1)} %get-tuple-element.4.mixer_in, bf16[128,2048]{1,0:T(8,128)(2,1)} %get-tuple-element.5.moe_in), custom_call_target="tpu_custom_call" | custom-call | tf_op jit(solution)/shard_map/pallas_call | solution.py:1173

commit v4 on v3

--- a/solution.py
+++ b/solution.py
@@ -729,6 +729,7 @@
     select(normed.at[row_peer], take(places_ref[row_peer], 0, 3), put_other)
 
     copy_n(1).start()
+    copy_n(2).start()
     fills = [
         pltpu.make_async_copy(packs.at[0], slots.at[0, own_blk], local_sem.at[4]),
         pltpu.make_async_copy(near_packs.at[0], slots.at[0, far_blk], local_sem.at[5]),
@@ -795,8 +796,6 @@
             def _(d):
                 copy_ah(d, half).start()
 
-        copy_n(2).start()
-
         @pl.when(low)
         def _():
             copy_k(near).start()
@@ -808,7 +807,8 @@
                 copy_k(d).start()
 
     def order(i):
-        return jnp.where(i < 2, i, jnp.where(i < near + 2, near - 2 + i, i - near))
+        later = jnp.where(i < near + 3, near - 3 + i, i - near)
+        return jnp.where(i < 2, i, jnp.where(i < 4, near - 2 + i, jnp.where(i == 4, 2, later)))
 
     def inside(j, low_bound):
         return jnp.logical_and(j >= low_bound, j < n)
@@ -1332,7 +1332,7 @@
     def body(*args):
         keys, moe_rows, routes = args[1], args[6], args[8]
         capacity = 2 * (moe_rows.shape[0] // tp_count) * routes.shape[1] // experts
-        whole_tiles = capacity % 16 == 0 and keys.shape[1] == 1
+        whole_tiles = capacity % 16 == 0 and keys.shape[1] == 1 and experts >= 8
         return (one_kernel if whole_tiles else local)(*args)
 
     return jax.shard_map(

time: 105 us -> 104 us (level)
  the two profiles are of different devices: /device:TPU:27 before, /device:TPU:0 now
where the time goes in v4:
time: 104 us
  Pallas kernels  103 us (99%)
    pallas_call x1, Pallas kernels, run_layer(): pl.pallas_call(functools.partial(layer_kernel, n), out_shape=(jax.ShapeDt...  101 us

profile of v4, /device:TPU:0, one launch (start us, length us, event | category | flops | bytes accessed | tf_op | source)
XLA Modules:
  0.0 103.5 jit_solution(10320557269428748600)
XLA Ops:
  0.6 100.9 %shard_map.140 = (bf16[64,2048]{1,0:T(8,128)(2,1)}, bf16[128,2048]{1,0:T(8,128)(2,1)}) custom-call(bf16[4,128,2048]{2,1,0:T(8,128)(2,1)} %bitcast.11, f32[1,2048]{1,0:T(1,128)} %bitcast.18, s32[2,512]{1,0:T(2,128)} %bitcast.19, f32[2,512]{1,0:T(2,128)} %bitcast.20, bf16[512,128]{1,0:T(8,128)(2,1)} %bitcast.15, bf16[256,128]{1,0:T(8,128)(2,1)} %bitcast.16, ...), custom_call_target="tpu_custom_call" | custom-call | flops 257698037760 | bytes 16777216 | tf_op jit(solution)/shard_map/pallas_call | solution.py:1123
  101.5 2.0 %shard_map.141 = (bf16[64,2048]{1,0:T(8,128)(2,1)}, bf16[128,2048]{1,0:T(8,128)(2,1)}) custom-call(bf16[64,2048]{1,0:T(8,128)(2,1)} %get-tuple-element.4.mixer_in, bf16[128,2048]{1,0:T(8,128)(2,1)} %get-tuple-element.5.moe_in), custom_call_target="tpu_custom_call" | custom-call | tf_op jit(solution)/shard_map/pallas_call | solution.py:1173
